TPU v7x, 32 devices: a whole 2x2x4 slice. The times are simulated.
32 devices in a mesh: sp: 4 (over z), fs: 4 (over y, x), tp: 2 (over core).
Axes of the slice: x: 2, y: 2, z: 4, core: 2. Of those that a mesh axis runs over, the one named last changes fastest.
Arguments:
- tokens: bfloat16 [4096, 2048], P(('fs', 'sp', 'tp')), parts along dimension 0, may hold values from -6 to 6
- norm_gain: float32 [2048], replicated, may hold values from 0.1 to 1.9
- recurrent_input: bfloat16 [2048, 1024], P(None, 'tp'), may hold values from -0.125 to 0.125
- recurrent_gate: bfloat16 [2048, 1024], P(None, 'tp'), may hold values from -0.125 to 0.125
- attention_gate: bfloat16 [2048, 1024], P(None, 'tp'), may hold values from -0.125 to 0.125
- query_proj: bfloat16 [2048, 1536], P(None, 'tp'), may hold values from -0.125 to 0.125
- latent_down: bfloat16 [2048, 512], P(None, 'tp'), may hold values from -0.125 to 0.125
- rope_key_down: bfloat16 [2048, 64], replicated, may hold values from -0.125 to 0.125
- conv_kernel: float32 [4, 1024], P(None, 'tp'), may hold values from -3 to 3
- recurrence_gate_blocks: bfloat16 [16, 64, 64], P('tp'), may hold values from -0.75 to 0.75
- input_gate_blocks: bfloat16 [16, 64, 64], P('tp'), may hold values from -0.75 to 0.75
- decay_rate: float32 [1024], P('tp'), as said below
- decay_shift: float32 [4096], P(('fs', 'sp')), parts along dimension 0, may hold values from -2 to 0, as said below
- initial_state: float32 [4096], P(('fs', 'tp')), parts along dimension 0, may hold values from -6 to 6
- latent_gain: float32 [512], replicated, may hold values from 0.1 to 1.9
- latent_up: bfloat16 [512, 2048], P(None, 'tp'), may hold values from -0.25 to 0.25
- query_gain: float32 [192], replicated, may hold values from 0.4 to 250, as said below
- recurrent_output: bfloat16 [1024, 2048], P('tp'), may hold values from -0.25 to 0.25
- attention_output: bfloat16 [1024, 2048], P('tp'), may hold values from -0.25 to 0.25
Outputs:
- mixed_output: bfloat16 [4096, 2048], P(('fs', 'sp', 'tp')), parts along dimension 0
There are 4 independent parts, one for each index of `fs`. A program takes and returns all parts, laid end to end along the dimension named above; an argument that names none is the same for every part. Nothing has to cross between parts.
Inputs may be any that keep to these rules, and one draw needn't show every extreme that they name: `decay_rate`: positive. `decay_shift`: negative. `query_gain`: positive.
All inputs are finite; a program needn't handle non-finite values.
Results may differ from a plain program's by a relative error of at most 0.03.
The roundings to bfloat16 on the way count: a program that leaves them out, or rounds other values in their place, can miss the bound.
Values may be sent and summed in bfloat16 or wider, within the bound.
A program may use at most 128 MiB of HBM per device.

v0:
```python
import functools

import jax
import jax.numpy as jnp
import numpy as np
from jax import lax
from jax.experimental import pallas as pl
from jax.experimental.pallas import tpu as pltpu
from jax.sharding import PartitionSpec as P

EPS = 1e-06
RECURRENT_SCALE = 8.0
THETA = 10000.0
F32 = jnp.float32
BF16 = jnp.bfloat16
LANES = 128


def expm1_neg(y):
    small = y * (1.0 + y * (0.5 + y * (1.0 / 6 + y * (1.0 / 24 + y * (1.0 / 120 + y / 720)))))
    return jnp.where(y > -0.35, small, jnp.exp(y) - 1.0)


def block_diagonal(scratch, blocks_ref, first):
    size = blocks_ref.shape[1]
    scratch[...] = jnp.zeros_like(scratch)
    for k in range(scratch.shape[0] // size):
        scratch[k * size : (k + 1) * size, k * size : (k + 1) * size] = blocks_ref[first + k]
    return scratch[...]


def scan_rows(decay, state):
    rows = decay.shape[0]
    row = lax.broadcasted_iota(jnp.int32, decay.shape, 0)
    step = 1
    while step < rows:
        inside = row >= step
        before_decay = jnp.where(inside, pltpu.roll(decay, step, 0), 1.0)
        before_state = jnp.where(inside, pltpu.roll(state, step, 0), 0.0)
        state = state + decay * before_state
        decay = decay * before_decay
        step *= 2
    return decay, state


def rms_scaled(values, gain_vec):
    return values * lax.rsqrt(jnp.mean(values * values, axis=-1, keepdims=True) + EPS) * gain_vec


LOG2E = 1.4426950408889634


def rotary_tables(positions, width):
    inv_freq = (1.0 / THETA ** (np.arange(0, width, 2, dtype=np.float32) / width)).astype(np.float32)
    angles = np.arange(positions, dtype=np.float32)[:, None] * inv_freq[None, :]
    cosine = np.cos(angles.astype(np.float64)).astype(np.float32)
    sine = np.sin(angles.astype(np.float64)).astype(np.float32)
    return cosine, sine


def column_step(width):
    return 256 if width % 256 == 0 else width


def remote(src, dst, send, recv, **where):
    return pltpu.make_async_remote_copy(
        src_ref=src, dst_ref=dst, send_sem=send, recv_sem=recv,
        device_id=where, device_id_type=pl.DeviceIdType.MESH,
    )


def scope(name):
    return jax.named_scope(name)


def layer_kernel(
    sp_count, tp_count,
    h_tokens, h_lat, h_norm, h_rope, h_ktab, h_in, h_query, h_qgain, h_qtab, h_conv, h_rec, h_inp,
    h_rate, h_shift, h_gate, h_att, h_lgain, h_up, h_init, h_rout, h_aout,
    out,
    tokens, w_lat, norm_gain, w_rope, key_table, w_in, w_query, query_gain, query_table,
    conv_kernel, rec_blocks, inp_blocks, decay_rate, decay_shift, w_gate, w_att, latent_gain,
    w_up, initial_state, w_rout, w_aout,
    tok_all, normed, lat_all, sig, gate, attp, turned_q, queries, rim_in, ext, diag_a, diag_b,
    prod, state, car_out, car_in, rout, racc, xlat, row_max, row_sum, acc, aout,
    part, own_part, part_in,
    w_sem, tok_s, tok_r, z_s, z_r, fwd_s, fwd_r, l_s, l_r, rim_s, rim_r, c_s, c_r, p_s, p_r, ready,
):
    sp = lax.axis_index("sp")
    tp = lax.axis_index("tp")
    share, model = tokens.shape
    rows = normed.shape[0]
    taps, width = conv_kernel.shape
    head_dim = query_gain.shape[1]
    rope = w_rope.shape[0]
    half = rope // 2
    nope = head_dim - rope
    heads = w_query.shape[1] // head_dim
    lat = w_lat.shape[1]
    value = w_att.shape[1] // heads
    packed = lat // rope
    tall = share // packed
    early = share + tall
    pieces = tok_s.shape[1]
    piece = share // pieces

    h_refs = (
        h_tokens, h_lat, h_norm, h_rope, h_ktab.at[sp * tp_count + tp], h_in, h_query, h_qgain,
        h_qtab.at[sp], h_conv, h_rec, h_inp, h_rate, h_shift, h_gate, h_att, h_lgain, h_up,
        h_init, h_rout, h_aout,
    )
    w_refs = (
        tokens, w_lat, norm_gain, w_rope, key_table, w_in, w_query, query_gain, query_table,
        conv_kernel, rec_blocks, inp_blocks, decay_rate, decay_shift, w_gate, w_att, latent_gain,
        w_up, initial_state, w_rout, w_aout,
    )
    loads = [
        pltpu.make_async_copy(a, b, w_sem.at[k]) for k, (a, b) in enumerate(zip(h_refs, w_refs))
    ]

    def peer(d):
        return lax.rem(tp + d, tp_count)

    def source(d):
        return lax.rem(tp - d + tp_count, tp_count)

    def greet(sem, **where):
        pl.semaphore_signal(sem, inc=1, device_id=where, device_id_type=pl.DeviceIdType.MESH)

    barrier = pltpu.get_barrier_semaphore()
    with scope("a_loads"):
        for d in range(1, tp_count):
            greet(barrier, tp=peer(d))
        for e in range(1, sp_count):
            pl.when(sp + e < sp_count)(lambda e=e: greet(barrier, sp=sp + e))
        for load in loads:
            load.start()
    (
        l_tok, l_lat, l_norm, l_rope, l_ktab, l_in, l_query, l_qgain, l_qtab, l_conv, l_rec, l_inp,
        l_rate, l_shift, l_gate, l_att, l_lgain, l_up, l_init, l_rout, l_aout,
    ) = loads

    def token_copy(d, k):
        part_rows = pl.ds(k * piece, piece)
        return remote(
            h_tokens.at[part_rows], tok_all.at[d - 1, part_rows],
            tok_s.at[d - 1, k], tok_r.at[d - 1, k], tp=peer(d),
        )

    with scope("b_barrier"):
        pl.semaphore_wait(barrier, tp_count - 1 + sp)
        for k in range(pieces):
            for d in range(1, tp_count):
                token_copy(d, k).start()
        for e in range(1, sp_count):
            pl.when(sp >= e)(lambda e=e: greet(ready.at[e - 1], sp=sp - e))

    def share_rows(place):
        return pl.ds(pl.multiple_of(place * share, share), share)

    def put_normed(block, place, k):
        first = pl.multiple_of(place * share + k * piece, piece)
        normed[pl.ds(first, piece)] = rms_scaled(block.astype(F32), norm_gain[...]).astype(BF16)

    def project(weight, into, here=slice(None)):
        step = column_step(weight.shape[1])
        for c in range(weight.shape[1] // step):
            cols = slice(c * step, (c + 1) * step)
            into[here, cols] = jnp.dot(
                normed[here], weight[:, cols], preferred_element_type=F32
            ).astype(BF16)

    own = lat_all.at[sp, tp]
    with scope("c_norm_own"):
        l_tok.wait()
        l_norm.wait()
        for k in range(pieces):
            put_normed(tokens[k * piece : (k + 1) * piece], tp, k)
    with scope("d_lat_a"):
        l_lat.wait()
        mine = normed[share_rows(tp)]
        own[:share] = jnp.dot(mine, w_lat[...], preferred_element_type=F32).astype(BF16)
        l_rope.wait()
        l_ktab.wait()
        raw = lax.dot_general(
            mine, w_rope[...], (((1,), (1,)), ((), ())), preferred_element_type=F32
        ).astype(BF16).astype(F32)
        swapped = jnp.concatenate([raw[:, half:], raw[:, :half]], axis=1)
        keyed = (raw * key_table[:, :rope] + swapped * key_table[:, rope:]).astype(BF16)
        for k in range(packed):
            own[share:early, k * rope : (k + 1) * rope] = keyed[k * tall : (k + 1) * tall]
    with scope("e_in_own"):
        l_in.wait()
        project(w_in, sig, share_rows(tp))

    def along(k):
        block = lat_all.at[sp, tp, (pl.ds(0, early), pl.ds(early, rows - share))[k]]
        return remote(block, block, z_s.at[k], z_r.at[k], sp=sp + 1)

    def landed(k):
        block = lat_all.at[sp - 1, tp, (pl.ds(0, early), pl.ds(early, rows - share))[k]]
        return remote(block, block, z_s.at[k], z_r.at[k], sp=sp - 1)

    def direct(e):
        block = lat_all.at[sp, tp]
        return remote(block, block, fwd_s.at[e - 2], fwd_r.at[e - 2], sp=sp + e)

    def forward():
        block = lat_all.at[sp - 1, tp]
        return remote(block, block, fwd_s.at[0], fwd_r.at[0], sp=sp + 1)

    def arrived(e):
        block = lat_all.at[sp - e, tp]
        return remote(block, block, fwd_s.at[e - 2], fwd_r.at[e - 2], sp=sp - 1)

    def across(e, d):
        block = lat_all.at[sp - e, tp]
        return remote(block, block, l_s.at[e, d - 1], l_r.at[e, d - 1], tp=peer(d))

    def crossed(e, d):
        block = lat_all.at[sp - e, source(d)]
        return remote(block, block, l_s.at[e, d - 1], l_r.at[e, d - 1], tp=source(d))

    def cross(e):
        for d in range(1, tp_count):
            across(e, d).start()

    def wait_crossed(e):
        for d in range(1, tp_count):
            crossed(e, d).wait_recv()

    has_next = sp + 1 < sp_count
    with scope("f_send_a"):

        @pl.when(has_next)
        def _():
            pl.semaphore_wait(ready.at[0], 1)
            along(0).start()

    with scope("g_norm_peer"):
        for k in range(pieces):
            for d in range(1, tp_count):
                token_copy(d, k).wait_recv()
                put_normed(tok_all[d - 1, k * piece : (k + 1) * piece], source(d), k)
    with scope("h_in_peer"):
        for d in range(1, tp_count):
            project(w_in, sig, share_rows(source(d)))

    def rim_copy():
        return remote(sig.at[pl.ds(rows - 16, 16)], rim_in, rim_s, rim_r, sp=sp + 1)

    def rim_landed():
        return remote(sig.at[pl.ds(rows - 16, 16)], rim_in, rim_s, rim_r, sp=sp - 1)

    with scope("i_lat_b"):
        pl.when(has_next)(lambda: rim_copy().start())
        for d in range(1, tp_count):
            own[early + (d - 1) * share : early + d * share] = jnp.dot(
                normed[share_rows(source(d))], w_lat[...], preferred_element_type=F32
            ).astype(BF16)
        pl.when(has_next)(lambda: along(1).start())
        cross(0)

    with scope("j_query"):
        l_query.wait()
        step = column_step(w_query.shape[1])
        for c in range(w_query.shape[1] // step):
            cols = slice(c * step, (c + 1) * step)
            raw = jnp.dot(normed[...], w_query[:, cols], preferred_element_type=F32).astype(BF16)
            turned_q[cols] = raw.T
    with scope("k_rotate"):
        l_qgain.wait()
        l_qtab.wait()
        spare = -head_dim % LANES
        gain = query_gain[...]
        if spare:
            gain = jnp.concatenate([gain, jnp.zeros((1, spare), F32)], axis=1)
        gain = jnp.broadcast_to(gain, (LANES, head_dim + spare)).T[:head_dim]
        gain = jnp.concatenate([gain] * (rows // LANES), axis=1)
        cosine = query_table[:half]
        sine = query_table[half:]
        for h in range(heads):
            head = turned_q[h * head_dim : (h + 1) * head_dim].astype(F32)
            square = jnp.sum(head * head, axis=0, keepdims=True)
            head = head * lax.rsqrt(square / head_dim + EPS) * gain
            first, second = head[nope : nope + half], head[nope + half :]
            queries[h, :nope] = head[:nope].astype(BF16)
            queries[h, nope : nope + half] = (first * cosine - second * sine).astype(BF16)
            queries[h, nope + half :] = (first * sine + second * cosine).astype(BF16)

    with scope("l_direct"):
        for e in range(2, sp_count):

            @pl.when(sp + e < sp_count)
            def _(e=e):
                pl.semaphore_wait(ready.at[e - 1], 1)
                if e > 2:
                    direct(e).start()

    with scope("m_rim"):

        @pl.when(sp == 0)
        def _():
            rim_in[...] = jnp.zeros_like(rim_in)

        pl.when(sp > 0)(lambda: rim_landed().wait_recv())
    with scope("n_scan"):
        for load in (l_conv, l_rec, l_inp, l_rate, l_shift):
            load.wait()
        ext[0:8] = rim_in[8:16].astype(F32)
        ext[8 : 8 + rows] = sig[...].astype(F32)
        size = rec_blocks.shape[1]
        car_out[...] = jnp.zeros_like(car_out)
        shift = jnp.broadcast_to(decay_shift[...], (LANES, rows)).T
        for c in range(width // LANES):
            cols = slice(c * LANES, (c + 1) * LANES)
            conv = conv_kernel[0:1, cols] * ext[9 - taps : 9 - taps + rows, cols]
            for j in range(1, taps):
                first = 9 - taps + j
                conv = conv + conv_kernel[j : j + 1, cols] * ext[first : first + rows, cols]
            conv = conv.astype(BF16)
            per = LANES // size
            rec = jax.nn.sigmoid(
                jnp.dot(conv, block_diagonal(diag_a, rec_blocks, c * per), preferred_element_type=F32)
            )
            inp = jax.nn.sigmoid(
                jnp.dot(conv, block_diagonal(diag_b, inp_blocks, c * per), preferred_element_type=F32)
            )
            log_decay = -RECURRENT_SCALE * rec * decay_rate[0:1, cols] + shift
            driven = jnp.sqrt(-expm1_neg(2.0 * log_decay)) * inp * conv.astype(F32)
            one, two = scan_rows(jnp.exp(log_decay), driven)
            prod[:, cols] = one
            state[:, cols] = two
            car_out[0:1, cols] = one[rows - 1 :]
            car_out[1:2, cols] = two[rows - 1 :]

    def carry_copy(e):
        return remote(car_out, car_in.at[e - 1], c_s.at[e - 1], c_r.at[e - 1], sp=sp + e)

    def carry_landed(e):
        return remote(car_out, car_in.at[e - 1], c_s.at[e - 1], c_r.at[e - 1], sp=sp - e)

    with scope("o_carry"):
        for e in range(1, sp_count):
            pl.when(sp + e < sp_count)(lambda e=e: carry_copy(e).start())
    with scope("p_relay1"):
        if sp_count > 1:

            @pl.when(sp >= 1)
            def _():
                landed(0).wait_recv()
                landed(1).wait_recv()
                if sp_count > 2:
                    pl.when(has_next)(lambda: forward().start())
                cross(1)

    with scope("q_gates"):
        l_gate.wait()
        project(w_gate, gate)
        l_att.wait()
        project(w_att, attp)

    factor = head_dim ** (-0.5) * LOG2E

    def attend(e, diagonal):
        place = sp - e
        blocks = []
        for n in range(tp_count):
            order = [(n - r) % tp_count for r in range(tp_count)]
            first = [0 if j == 0 else early + (j - 1) * share for j in order]
            blocks.append(
                jnp.concatenate([lat_all[place, n, f : f + share] for f in first], axis=0).astype(F32)
            )
        square = sum(jnp.sum(x * x, axis=-1, keepdims=True) for x in blocks)
        inverse = lax.rsqrt(square / (lat * tp_count) + EPS)
        for n, x in enumerate(blocks):
            cols = slice(n * lat, (n + 1) * lat)
            xlat[:, cols] = (x * inverse * latent_gain[0:1, cols]).astype(BF16)
        turned = jnp.concatenate(
            [
                lat_all[place, n, share:early, k * rope : (k + 1) * rope]
                for n in range(tp_count)
                for k in range(packed)
            ],
            axis=0,
        )
        for h in range(heads):
            base = h * (nope + value)
            kv = jnp.dot(
                xlat[...], w_up[:, base : base + nope + value], preferred_element_type=F32
            ).astype(BF16)
            keys = jnp.concatenate([kv[:, :nope], turned], axis=1)
            scores = jnp.dot(keys, queries[h], preferred_element_type=F32) * factor
            if diagonal:
                seen = lax.broadcasted_iota(jnp.int32, scores.shape, 0)
                scores = jnp.where(
                    seen <= lax.broadcasted_iota(jnp.int32, scores.shape, 1), scores, -jnp.inf
                )
            top = jnp.max(scores, axis=0, keepdims=True)
            if not diagonal:
                before = row_max[h, 0:1]
                top = jnp.maximum(top, before)
                fade = jnp.exp2(before - top)
            weights = jnp.exp2(scores - top)
            mass = jnp.sum(weights, axis=0, keepdims=True)
            term = jnp.dot(
                kv[:, nope:].T, weights.astype(BF16), preferred_element_type=F32
            )
            if not diagonal:
                mass = mass + row_sum[h, 0:1] * fade
                term = term + acc[h] * fade
            row_max[h, 0:1] = top
            row_sum[h, 0:1] = mass
            acc[h] = term

    with scope("r_att0"):
        l_lgain.wait()
        l_up.wait()
        wait_crossed(0)
        attend(0, True)
    with scope("s_att1"):
        if sp_count > 1:

            @pl.when(sp >= 1)
            def _():
                wait_crossed(1)
                attend(1, False)

    with scope("t_relay3"):
        if sp_count > 3:

            @pl.when(sp >= 3)
            def _():
                arrived(3).wait_recv()
                cross(3)

    with scope("u_carrywait"):
        for e in range(1, sp_count):

            @pl.when(sp >= e)
            def _(e=e):
                carry_landed(e).wait_recv()

            @pl.when(sp < e)
            def _(e=e):
                car_in[e - 1, 0:1] = jnp.ones((1, width), F32)
                car_in[e - 1, 1:2] = jnp.zeros((1, width), F32)

    with scope("v_rout"):
        l_init.wait()
        incoming = initial_state[...]
        for e in range(sp_count - 1, 0, -1):
            incoming = car_in[e - 1, 0:1] * incoming + car_in[e - 1, 1:2]
        for c in range(width // LANES):
            cols = slice(c * LANES, (c + 1) * LANES)
            full = state[:, cols] + prod[:, cols] * incoming[:, cols]
            rout[:, cols] = (full * jax.nn.silu(gate[:, cols].astype(F32))).astype(BF16)
        l_rout.wait()
        step = column_step(model)
        for c in range(model // step):
            cols = slice(c * step, (c + 1) * step)
            racc[:, cols] = jnp.dot(rout[...], w_rout[:, cols], preferred_element_type=F32)
    with scope("w_att3"):
        if sp_count > 3:

            @pl.when(sp >= 3)
            def _():
                wait_crossed(3)
                attend(3, False)

        if sp_count > 4:

            def later(e, carry):
                block = lat_all.at[sp - e, tp]
                remote(block, block, fwd_s.at[e - 2], fwd_r.at[e - 2], sp=sp - 1).wait_recv()
                cross(e)
                wait_crossed(e)
                attend(e, False)
                return carry

            lax.fori_loop(4, sp + 1, later, 0)
    with scope("x_relay2"):
        if sp_count > 2:

            @pl.when(sp >= 2)
            def _():
                arrived(2).wait_recv()
                cross(2)
                wait_crossed(2)

    with scope("y_att2"):
        if sp_count > 2:
            pl.when(sp >= 2)(lambda: attend(2, False))
    with scope("z_aout"):
        for h in range(heads):
            cols = slice(h * value, (h + 1) * value)
            attended = (acc[h] * (1.0 / row_sum[h, 0:1])).T
            aout[:, cols] = (attended * jax.nn.silu(attp[:, cols].astype(F32))).astype(BF16)

    chunks, step = part.shape[1], part.shape[3]

    def part_copy(d, c):
        return remote(
            part.at[d - 1, c], part_in.at[d - 1, c], p_s.at[d - 1, c], p_r.at[d - 1, c], tp=peer(d)
        )

    def partial(place, c):
        cols = slice(c * step, (c + 1) * step)
        here = share_rows(place)
        both = racc[here, cols] + jnp.dot(aout[here], w_aout[:, cols], preferred_element_type=F32)
        return both.astype(BF16)

    with scope("z_outmm"):
        l_aout.wait()
        for c in range(chunks):
            for d in range(1, tp_count):
                part[d - 1, c] = partial(peer(d), c)
                part_copy(d, c).start()
        for c in range(chunks):
            own_part[c] = partial(tp, c)
    with scope("z_sum"):
        for c in range(chunks):
            summed = own_part[c].astype(F32)
            for d in range(1, tp_count):
                part_copy(d, c).wait_recv()
                summed = summed + part_in[d - 1, c].astype(F32)
            out[:, c * step : (c + 1) * step] = summed.astype(BF16)

    with scope("z_waits"):
        for d in range(1, tp_count):
            for k in range(pieces):
                token_copy(d, k).wait_send()
            for c in range(chunks):
                part_copy(d, c).wait_send()
            across(0, d).wait_send()

        @pl.when(has_next)
        def _():
            rim_copy().wait_send()
            along(0).wait_send()
            along(1).wait_send()

        for e in range(1, sp_count):

            @pl.when(sp + e < sp_count)
            def _(e=e):
                carry_copy(e).wait_send()
                if e > 2:
                    direct(e).wait_send()

            @pl.when(sp >= e)
            def _(e=e):
                for d in range(1, tp_count):
                    across(e, d).wait_send()

        if sp_count > 2:
            pl.when((sp >= 1) & has_next)(lambda: forward().wait_send())


def body(
    tokens, norm_gain, recurrent_input, recurrent_gate, attention_gate, query_proj, latent_down,
    rope_key_down, conv_kernel, recurrence_gate_blocks, input_gate_blocks, decay_rate, decay_shift,
    initial_state, latent_gain, latent_up, query_gain, recurrent_output, attention_output,
):
    tp_count = lax.axis_size("tp")
    sp_count = lax.axis_size("sp")
    share, model = tokens.shape
    rows = share * tp_count
    width = recurrent_input.shape[1]
    taken = attention_gate.shape[1]
    head_dim = query_gain.shape[0]
    heads = query_proj.shape[1] // head_dim
    value = taken // heads
    lat = latent_down.shape[1]
    rope = rope_key_down.shape[1]
    cosine, sine = rotary_tables(sp_count * rows, rope)
    key_table = np.concatenate([cosine, cosine, -sine, sine], 1).reshape(-1, share, 2 * rope)
    query_table = np.concatenate([cosine, sine], 1).reshape(sp_count, rows, rope).transpose(0, 2, 1)
    hbm = [
        tokens, latent_down, norm_gain[None], rope_key_down.T, jnp.asarray(key_table),
        recurrent_input, query_proj, query_gain[None], jnp.asarray(query_table), conv_kernel,
        recurrence_gate_blocks, input_gate_blocks, decay_rate[None], decay_shift[None],
        recurrent_gate, attention_gate, latent_gain[None], latent_up, initial_state[None],
        recurrent_output, attention_output,
    ]
    held = [a.shape for a in hbm]
    held[4] = key_table.shape[1:]
    held[8] = query_table.shape[1:]
    vmem = pltpu.VMEM
    dma = pltpu.SemaphoreType.DMA
    others = max(tp_count - 1, 1)
    hops = max(sp_count - 1, 1)
    pieces = 4 if share % 64 == 0 else 1
    chunks = 4 if model % (4 * LANES) == 0 else 1
    return pl.pallas_call(
        functools.partial(layer_kernel, sp_count, tp_count),
        out_shape=pltpu.VMEM((share, model), BF16),
        in_specs=[pl.BlockSpec(memory_space=pl.ANY)] * len(hbm),
        out_specs=pl.BlockSpec(memory_space=pltpu.VMEM),
        scratch_shapes=[vmem(s, a.dtype) for s, a in zip(held, hbm)]
        + [
            vmem((others, share, model), BF16),
            vmem((rows, model), BF16),
            vmem((sp_count, tp_count, rows + share * rope // lat, lat), BF16),
            vmem((rows, width), BF16),
            vmem((rows, width), BF16),
            vmem((rows, taken), BF16),
            vmem((query_proj.shape[1], rows), BF16),
            vmem((heads, head_dim, rows), BF16),
            vmem((16, width), BF16),
            vmem((rows + 8, width), F32),
            vmem((LANES, LANES), BF16),
            vmem((LANES, LANES), BF16),
            vmem((rows, width), F32),
            vmem((rows, width), F32),
            vmem((8, width), F32),
            vmem((hops, 8, width), F32),
            vmem((rows, width), BF16),
            vmem((rows, model), F32),
            vmem((rows, lat * tp_count), BF16),
            vmem((heads, 8, rows), F32),
            vmem((heads, 8, rows), F32),
            vmem((heads, value, rows), F32),
            vmem((rows, taken), BF16),
            vmem((others, chunks, share, model // chunks), BF16),
            vmem((chunks, share, model // chunks), BF16),
            vmem((others, chunks, share, model // chunks), BF16),
            dma((len(hbm),)),
            dma((others, pieces)), dma((others, pieces)),
            dma((2,)), dma((2,)),
            dma((hops,)), dma((hops,)),
            dma((sp_count, others)), dma((sp_count, others)),
            dma, dma,
            dma((hops,)), dma((hops,)),
            dma((others, chunks)), dma((others, chunks)),
            pltpu.SemaphoreType.REGULAR((hops,)),
        ],
        compiler_params=pltpu.CompilerParams(
            collective_id=0, has_side_effects=True, vmem_limit_bytes=61400 * 1024
        ),
    )(*hbm)


def solution(mesh):
    return jax.shard_map(
        body,
        mesh=mesh,
        in_specs=(
            P(("fs", "sp", "tp"), None),
            P(),
            P(None, "tp"),
            P(None, "tp"),
            P(None, "tp"),
            P(None, "tp"),
            P(None, "tp"),
            P(),
            P(None, "tp"),
            P("tp", None, None),
            P("tp", None, None),
            P("tp"),
            P(("fs", "sp")),
            P(("fs", "tp")),
            P(),
            P(None, "tp"),
            P(),
            P("tp", None),
            P("tp", None),
        ),
        out_specs=P(("fs", "sp", "tp"), None),
        check_vma=False,
    )
```

profile of v0, /device:TPU:25, one launch (start us, length us, event | category | flops | bytes accessed | tf_op | source)
XLA Modules:
  0.0 27.6 jit_solution(470319156621411653)
XLA Ops:
  0.0 26.8 %shard_map.199 = bf16[128,2048]{1,0:T(8,128)(2,1)S(1)} custom-call(bf16[128,2048]{1,0:T(8,128)(2,1)} %h_tokens.1, bf16[2048,256]{1,0:T(8,128)(2,1)} %h_lat.1, f32[1,2048]{1,0:T(1,128)} %bitcast.8, bf16[64,2048]{1,0:T(8,128)(2,1)} %bitcast.7, f32[8,128,128]{2,1,0:T(8,128)} %constant.4.clone.h_ktab, bf16[2048,512]{1,0:T(8,128)(2,1)} %h_in.1, ...), custom_call_target="tpu_custom_call" | custom-call | tf_op jit(solution)/shard_map/pallas_call | solution.py:595
  26.8 0.8 %copy.23 = bf16[128,2048]{1,0:T(8,128)(2,1)} copy(bf16[128,2048]{1,0:T(8,128)(2,1)S(1)} %shard_map.199) | data formatting | bytes 1048576
where the time goes:
time: 27.7 us; the launch traced here: 27.6 us
  Pallas kernels  26.8 us (97%)
  local copies, waits for them, and re-layouts  0.8 us (3%)
    pallas_call x1, Pallas kernels, body(): pl.pallas_call(functools.partial(layer_kernel, sp_count, tp_count), out_s...  26.8 us
    unnamed x1, local copies, waits for them, and re-layouts  0.8 us

commit v1 on v0

--- a/solution.py
+++ b/solution.py
@@ -16,9 +16,9 @@
 LANES = 128
 
 
-def expm1_neg(y):
-    small = y * (1.0 + y * (0.5 + y * (1.0 / 6 + y * (1.0 / 24 + y * (1.0 / 120 + y / 720)))))
-    return jnp.where(y > -0.35, small, jnp.exp(y) - 1.0)
+def expm1_neg(y, root):
+    small = y * (1.0 + y * (0.5 + y * (1.0 / 6 + y * (1.0 / 24 + y / 120))))
+    return jnp.where(y > -0.1, small, root * root - 1.0)
 
 
 def block_diagonal(scratch, blocks_ref, first):
@@ -81,10 +81,12 @@
     tokens, w_lat, norm_gain, w_rope, key_table, w_in, w_query, query_gain, query_table,
     conv_kernel, rec_blocks, inp_blocks, decay_rate, decay_shift, w_gate, w_att, latent_gain,
     w_up, initial_state, w_rout, w_aout,
-    tok_all, normed, lat_all, sig, gate, attp, turned_q, queries, rim_in, ext, diag_a, diag_b,
-    prod, state, car_out, car_in, rout, racc, xlat, row_max, row_sum, acc, aout,
-    part, own_part, part_in,
-    w_sem, tok_s, tok_r, z_s, z_r, fwd_s, fwd_r, l_s, l_r, rim_s, rim_r, c_s, c_r, p_s, p_r, ready,
+    tok_all, normed, lat_all, sig, gate, attp, turned_q, queries, rim_out, rim_in, ext, diag_a, diag_b,
+    mixer, unmixer, shift, silu_gate, mixed_rout,
+    prod, state, segments, car_out, car_in, rout, racc, xlat, rope_keys, kv, held, row_max, row_sum,
+    acc, aout, part, own_part, part_in,
+    w_sem, tok_sem, tok_s, tok_r, z_s, z_r, y_s, y_r, fwd_s, fwd_r, l_s, l_r, rim_s, rim_r, c_s, c_r,
+    p_s, p_r, ready,
 ):
     sp = lax.axis_index("sp")
     tp = lax.axis_index("tp")
@@ -100,9 +102,9 @@
     value = w_att.shape[1] // heads
     packed = lat // rope
     tall = share // packed
-    early = share + tall
     pieces = tok_s.shape[1]
     piece = share // pieces
+    long = rows // 8
 
     h_refs = (
         h_tokens, h_lat, h_norm, h_rope, h_ktab.at[sp * tp_count + tp], h_in, h_query, h_qgain,
@@ -115,7 +117,13 @@
         w_up, initial_state, w_rout, w_aout,
     )
     loads = [
-        pltpu.make_async_copy(a, b, w_sem.at[k]) for k, (a, b) in enumerate(zip(h_refs, w_refs))
+        pltpu.make_async_copy(a, b, w_sem.at[k]) for k, (a, b) in enumerate(zip(h_refs, w_refs)) if k
+    ]
+    token_loads = [
+        pltpu.make_async_copy(
+            h_tokens.at[pl.ds(k * piece, piece)], tokens.at[pl.ds(k * piece, piece)], tok_sem.at[k]
+        )
+        for k in range(pieces)
     ]
 
     def peer(d):
@@ -133,10 +141,10 @@
             greet(barrier, tp=peer(d))
         for e in range(1, sp_count):
             pl.when(sp + e < sp_count)(lambda e=e: greet(barrier, sp=sp + e))
-        for load in loads:
+        for load in [loads[1], *token_loads, loads[0]]:
             load.start()
     (
-        l_tok, l_lat, l_norm, l_rope, l_ktab, l_in, l_query, l_qgain, l_qtab, l_conv, l_rec, l_inp,
+        l_lat, l_norm, l_rope, l_ktab, l_in, l_query, l_qgain, l_qtab, l_conv, l_rec, l_inp,
         l_rate, l_shift, l_gate, l_att, l_lgain, l_up, l_init, l_rout, l_aout,
     ) = loads
 
@@ -154,13 +162,19 @@
                 token_copy(d, k).start()
         for e in range(1, sp_count):
             pl.when(sp >= e)(lambda e=e: greet(ready.at[e - 1], sp=sp - e))
+        for load in (loads[2], loads[3], loads[4], loads[5]):
+            load.start()
 
     def share_rows(place):
         return pl.ds(pl.multiple_of(place * share, share), share)
 
-    def put_normed(block, place, k):
-        first = pl.multiple_of(place * share + k * piece, piece)
-        normed[pl.ds(first, piece)] = rms_scaled(block.astype(F32), norm_gain[...]).astype(BF16)
+    def put_normed(block, place):
+        normed[share_rows(place)] = rms_scaled(block.astype(F32), norm_gain[...]).astype(BF16)
+
+    def put_latent(first, place):
+        own[first : first + share] = jnp.dot(
+            normed[share_rows(place)], w_lat[...], preferred_element_type=F32
+        ).astype(BF16)
 
     def project(weight, into, here=slice(None)):
         step = column_step(weight.shape[1])
@@ -172,95 +186,111 @@
 
     own = lat_all.at[sp, tp]
     with scope("c_norm_own"):
-        l_tok.wait()
         l_norm.wait()
         for k in range(pieces):
-            put_normed(tokens[k * piece : (k + 1) * piece], tp, k)
+            token_loads[k].wait()
+        put_normed(tokens[...], tp)
     with scope("d_lat_a"):
         l_lat.wait()
-        mine = normed[share_rows(tp)]
-        own[:share] = jnp.dot(mine, w_lat[...], preferred_element_type=F32).astype(BF16)
+        put_latent(0, tp)
+
+    def along(k):
+        block = lat_all.at[sp, tp, (pl.ds(0, share), pl.ds(share, rows + tall - share))[k]]
+        return remote(block, block, z_s.at[k], z_r.at[k], sp=sp + 1)
+
+    def landed(k):
+        block = lat_all.at[sp - 1, tp, (pl.ds(0, share), pl.ds(share, rows + tall - share))[k]]
+        return remote(block, block, z_s.at[k], z_r.at[k], sp=sp - 1)
+
+    def direct(e):
+        block = lat_all.at[sp, tp]
+        return remote(block, block, fwd_s.at[e - 2], fwd_r.at[e - 2], sp=sp + e)
+
+    def forward(k):
+        block = lat_all.at[sp - 1, tp, (pl.ds(0, share), pl.ds(share, rows + tall - share))[k]]
+        return remote(block, block, y_s.at[k], y_r.at[k], sp=sp + 1)
+
+    def forwarded(k):
+        block = lat_all.at[sp - 2, tp, (pl.ds(0, share), pl.ds(share, rows + tall - share))[k]]
+        return remote(block, block, y_s.at[k], y_r.at[k], sp=sp - 1)
+
+    def arrived(e):
+        block = lat_all.at[sp - e, tp]
+        return remote(block, block, fwd_s.at[e - 2], fwd_r.at[e - 2], sp=sp - 1)
+
+    def across(e, d):
+        block = lat_all.at[sp - e, tp]
+        return remote(block, block, l_s.at[e, d - 1], l_r.at[e, d - 1], tp=peer(d))
+
+    def crossed(e, d):
+        block = lat_all.at[sp - e, source(d)]
+        return remote(block, block, l_s.at[e, d - 1], l_r.at[e, d - 1], tp=source(d))
+
+    def cross(e):
+        for d in range(1, tp_count):
+            across(e, d).start()
+
+    def wait_crossed(e):
+        for d in range(1, tp_count):
+            crossed(e, d).wait_recv()
+
+    has_next = sp + 1 < sp_count
+    with scope("f_send_a"):
+
+        @pl.when(has_next)
+        def _():
+            pl.semaphore_wait(ready.at[0], 1)
+            along(0).start()
+
+    with scope("e_mixers"):
+        row = lax.broadcasted_iota(jnp.int32, (rows, rows), 0)
+        column = lax.broadcasted_iota(jnp.int32, (rows, rows), 1)
+        mixer[...] = jnp.where(column == (row & 7) * long + (row >> 3), 1.0, 0.0).astype(BF16)
+        unmixer[...] = jnp.where(row == (column & 7) * long + (column >> 3), 1.0, 0.0).astype(BF16)
+    with scope("e_rope"):
         l_rope.wait()
         l_ktab.wait()
         raw = lax.dot_general(
-            mine, w_rope[...], (((1,), (1,)), ((), ())), preferred_element_type=F32
+            normed[share_rows(tp)], w_rope[...], (((1,), (1,)), ((), ())),
+            preferred_element_type=F32,
         ).astype(BF16).astype(F32)
         swapped = jnp.concatenate([raw[:, half:], raw[:, :half]], axis=1)
         keyed = (raw * key_table[:, :rope] + swapped * key_table[:, rope:]).astype(BF16)
         for k in range(packed):
-            own[share:early, k * rope : (k + 1) * rope] = keyed[k * tall : (k + 1) * tall]
+            own[share : share + tall, k * rope : (k + 1) * rope] = keyed[k * tall : (k + 1) * tall]
     with scope("e_in_own"):
+        for load in loads[6:8]:
+            load.start()
         l_in.wait()
         project(w_in, sig, share_rows(tp))
-
-    def along(k):
-        block = lat_all.at[sp, tp, (pl.ds(0, early), pl.ds(early, rows - share))[k]]
-        return remote(block, block, z_s.at[k], z_r.at[k], sp=sp + 1)
-
-    def landed(k):
-        block = lat_all.at[sp - 1, tp, (pl.ds(0, early), pl.ds(early, rows - share))[k]]
-        return remote(block, block, z_s.at[k], z_r.at[k], sp=sp - 1)
-
-    def direct(e):
-        block = lat_all.at[sp, tp]
-        return remote(block, block, fwd_s.at[e - 2], fwd_r.at[e - 2], sp=sp + e)
-
-    def forward():
-        block = lat_all.at[sp - 1, tp]
-        return remote(block, block, fwd_s.at[0], fwd_r.at[0], sp=sp + 1)
-
-    def arrived(e):
-        block = lat_all.at[sp - e, tp]
-        return remote(block, block, fwd_s.at[e - 2], fwd_r.at[e - 2], sp=sp - 1)
-
-    def across(e, d):
-        block = lat_all.at[sp - e, tp]
-        return remote(block, block, l_s.at[e, d - 1], l_r.at[e, d - 1], tp=peer(d))
-
-    def crossed(e, d):
-        block = lat_all.at[sp - e, source(d)]
-        return remote(block, block, l_s.at[e, d - 1], l_r.at[e, d - 1], tp=source(d))
-
-    def cross(e):
-        for d in range(1, tp_count):
-            across(e, d).start()
-
-    def wait_crossed(e):
-        for d in range(1, tp_count):
-            crossed(e, d).wait_recv()
-
-    has_next = sp + 1 < sp_count
-    with scope("f_send_a"):
-
-        @pl.when(has_next)
-        def _():
-            pl.semaphore_wait(ready.at[0], 1)
-            along(0).start()
-
     with scope("g_norm_peer"):
         for k in range(pieces):
             for d in range(1, tp_count):
                 token_copy(d, k).wait_recv()
-                put_normed(tok_all[d - 1, k * piece : (k + 1) * piece], source(d), k)
+        for d in range(1, tp_count):
+            put_normed(tok_all[d - 1], source(d))
+    def rim_copy():
+        return remote(rim_out, rim_in, rim_s, rim_r, sp=sp + 1)
+
+    def rim_landed():
+        return remote(rim_out, rim_in, rim_s, rim_r, sp=sp - 1)
+
     with scope("h_in_peer"):
+        for load in loads[8:]:
+            load.start()
         for d in range(1, tp_count):
             project(w_in, sig, share_rows(source(d)))
-
-    def rim_copy():
-        return remote(sig.at[pl.ds(rows - 16, 16)], rim_in, rim_s, rim_r, sp=sp + 1)
-
-    def rim_landed():
-        return remote(sig.at[pl.ds(rows - 16, 16)], rim_in, rim_s, rim_r, sp=sp - 1)
-
+        tail = sig[rows - 16 :].astype(F32)[12:]
+        tail = [tail[:, c * LANES : (c + 1) * LANES] for c in range(width // LANES)]
+        if len(tail) * 4 < rim_out.shape[0]:
+            tail.append(jnp.zeros((rim_out.shape[0] - len(tail) * 4, LANES), F32))
+        rim_out[...] = jnp.concatenate(tail, axis=0).astype(BF16)
+        pl.when(has_next)(lambda: rim_copy().start())
     with scope("i_lat_b"):
-        pl.when(has_next)(lambda: rim_copy().start())
         for d in range(1, tp_count):
-            own[early + (d - 1) * share : early + d * share] = jnp.dot(
-                normed[share_rows(source(d))], w_lat[...], preferred_element_type=F32
-            ).astype(BF16)
+            put_latent(d * share + tall, source(d))
         pl.when(has_next)(lambda: along(1).start())
         cross(0)
-
     with scope("j_query"):
         l_query.wait()
         step = column_step(w_query.shape[1])
@@ -307,17 +337,31 @@
     with scope("n_scan"):
         for load in (l_conv, l_rec, l_inp, l_rate, l_shift):
             load.wait()
-        ext[0:8] = rim_in[8:16].astype(F32)
-        ext[8 : 8 + rows] = sig[...].astype(F32)
         size = rec_blocks.shape[1]
         car_out[...] = jnp.zeros_like(car_out)
-        shift = jnp.broadcast_to(decay_shift[...], (LANES, rows)).T
-        for c in range(width // LANES):
+        lead = 8 * (taps - 1)
+        ext[lead : lead + rows] = jnp.dot(mixer[...], sig[...], preferred_element_type=F32)
+        top_row = lax.broadcasted_iota(jnp.int32, (8, width), 0) == 0
+        rim = rim_in[...].astype(F32)
+        rim = jnp.concatenate(
+            [rim[4 * c : 4 * c + 4] for c in range(width // LANES)], axis=1
+        )
+        for k in range(1, taps):
+            last = ext[lead + rows - 8 * k : lead + rows - 8 * k + 8]
+            ext[lead - 8 * k : lead - 8 * k + 8] = jnp.where(
+                top_row, rim[4 - k : 5 - k], pltpu.roll(last, 1, 0)
+            )
+        table = jnp.concatenate(
+            [decay_shift[:, k * long : (k + 1) * long] for k in range(8)], axis=0
+        )
+        for i in range(long):
+            shift[8 * i : 8 * i + 8] = jnp.broadcast_to(table[:, i : i + 1], (8, LANES))
+        groups = width // LANES
+        for c in range(groups):
             cols = slice(c * LANES, (c + 1) * LANES)
-            conv = conv_kernel[0:1, cols] * ext[9 - taps : 9 - taps + rows, cols]
+            conv = conv_kernel[0:1, cols] * ext[0:rows, cols]
             for j in range(1, taps):
-                first = 9 - taps + j
-                conv = conv + conv_kernel[j : j + 1, cols] * ext[first : first + rows, cols]
+                conv = conv + conv_kernel[j : j + 1, cols] * ext[8 * j : 8 * j + rows, cols]
             conv = conv.astype(BF16)
             per = LANES // size
             rec = jax.nn.sigmoid(
@@ -326,13 +370,28 @@
             inp = jax.nn.sigmoid(
                 jnp.dot(conv, block_diagonal(diag_b, inp_blocks, c * per), preferred_element_type=F32)
             )
-            log_decay = -RECURRENT_SCALE * rec * decay_rate[0:1, cols] + shift
-            driven = jnp.sqrt(-expm1_neg(2.0 * log_decay)) * inp * conv.astype(F32)
-            one, two = scan_rows(jnp.exp(log_decay), driven)
-            prod[:, cols] = one
-            state[:, cols] = two
-            car_out[0:1, cols] = one[rows - 1 :]
-            car_out[1:2, cols] = two[rows - 1 :]
+            log_decay = -RECURRENT_SCALE * rec * decay_rate[0:1, cols] + shift[...]
+            decay = jnp.exp(log_decay)
+            prod[c] = decay
+            state[c] = jnp.sqrt(-expm1_neg(2.0 * log_decay, decay)) * inp * conv.astype(F32)
+        ones = [prod[c, 0:8] for c in range(groups)]
+        twos = [state[c, 0:8] for c in range(groups)]
+        for i in range(1, long):
+            here = slice(8 * i, 8 * i + 8)
+            for c in range(groups):
+                decay = prod[c, here]
+                twos[c] = decay * twos[c] + state[c, here]
+                ones[c] = decay * ones[c]
+                prod[c, here] = ones[c]
+                state[c, here] = twos[c]
+        first_row = lax.broadcasted_iota(jnp.int32, (8, LANES), 0) == 0
+        for c in range(groups):
+            cols = slice(c * LANES, (c + 1) * LANES)
+            one, two = scan_rows(ones[c], twos[c])
+            segments[0:8, cols] = jnp.where(first_row, 1.0, pltpu.roll(one, 1, 0))
+            segments[8:16, cols] = jnp.where(first_row, 0.0, pltpu.roll(two, 1, 0))
+            car_out[2 * c : 2 * c + 1] = one[7:8]
+            car_out[2 * c + 1 : 2 * c + 2] = two[7:8]
 
     def carry_copy(e):
         return remote(car_out, car_in.at[e - 1], c_s.at[e - 1], c_r.at[e - 1], sp=sp + e)
@@ -343,31 +402,37 @@
     with scope("o_carry"):
         for e in range(1, sp_count):
             pl.when(sp + e < sp_count)(lambda e=e: carry_copy(e).start())
-    with scope("p_relay1"):
+    def relay1(k):
         if sp_count > 1:
 
             @pl.when(sp >= 1)
             def _():
-                landed(0).wait_recv()
-                landed(1).wait_recv()
+                landed(k).wait_recv()
                 if sp_count > 2:
-                    pl.when(has_next)(lambda: forward().start())
-                cross(1)
+                    pl.when(has_next)(lambda: forward(k).start())
+                if k:
+                    cross(1)
+
+    with scope("p_relay1a"):
+        relay1(0)
 
     with scope("q_gates"):
         l_gate.wait()
         project(w_gate, gate)
         l_att.wait()
         project(w_att, attp)
+        silu_gate[...] = jax.nn.silu(
+            jnp.dot(mixer[...], gate[...], preferred_element_type=F32)
+        )
 
     factor = head_dim ** (-0.5) * LOG2E
 
-    def attend(e, diagonal):
+    def prepare(e):
         place = sp - e
         blocks = []
         for n in range(tp_count):
             order = [(n - r) % tp_count for r in range(tp_count)]
-            first = [0 if j == 0 else early + (j - 1) * share for j in order]
+            first = [0 if j == 0 else tall + j * share for j in order]
             blocks.append(
                 jnp.concatenate([lat_all[place, n, f : f + share] for f in first], axis=0).astype(F32)
             )
@@ -376,48 +441,80 @@
         for n, x in enumerate(blocks):
             cols = slice(n * lat, (n + 1) * lat)
             xlat[:, cols] = (x * inverse * latent_gain[0:1, cols]).astype(BF16)
-        turned = jnp.concatenate(
+        rope_keys[...] = jnp.concatenate(
             [
-                lat_all[place, n, share:early, k * rope : (k + 1) * rope]
+                lat_all[place, n, share : share + tall, k * rope : (k + 1) * rope]
                 for n in range(tp_count)
                 for k in range(packed)
             ],
             axis=0,
         )
-        for h in range(heads):
+        step = column_step(w_up.shape[1])
+        for c in range(w_up.shape[1] // step):
+            cols = slice(c * step, (c + 1) * step)
+            kv[:, cols] = jnp.dot(xlat[...], w_up[:, cols], preferred_element_type=F32).astype(BF16)
+
+    def heads_over(diagonal, lanes=slice(None), count=None):
+        count = rows if count is None else count
+
+        def score(h):
             base = h * (nope + value)
-            kv = jnp.dot(
-                xlat[...], w_up[:, base : base + nope + value], preferred_element_type=F32
-            ).astype(BF16)
-            keys = jnp.concatenate([kv[:, :nope], turned], axis=1)
-            scores = jnp.dot(keys, queries[h], preferred_element_type=F32) * factor
+            keys = jnp.concatenate([kv[:, base : base + nope], rope_keys[...]], axis=1)
+            scores = jnp.dot(keys, queries[h, :, lanes], preferred_element_type=F32) * factor
             if diagonal:
                 seen = lax.broadcasted_iota(jnp.int32, scores.shape, 0)
                 scores = jnp.where(
                     seen <= lax.broadcasted_iota(jnp.int32, scores.shape, 1), scores, -jnp.inf
                 )
-            top = jnp.max(scores, axis=0, keepdims=True)
+            held[h, :, :count] = scores
+            return jnp.max(scores, axis=0, keepdims=True)
+
+        def mix(h, top):
+            base = h * (nope + value) + nope
             if not diagonal:
-                before = row_max[h, 0:1]
+                before = row_max[h, 0:1, lanes]
                 top = jnp.maximum(top, before)
                 fade = jnp.exp2(before - top)
-            weights = jnp.exp2(scores - top)
+            weights = jnp.exp2(held[h, :, :count] - top)
             mass = jnp.sum(weights, axis=0, keepdims=True)
             term = jnp.dot(
-                kv[:, nope:].T, weights.astype(BF16), preferred_element_type=F32
+                kv[:, base : base + value].T, weights.astype(BF16), preferred_element_type=F32
             )
             if not diagonal:
-                mass = mass + row_sum[h, 0:1] * fade
-                term = term + acc[h] * fade
-            row_max[h, 0:1] = top
-            row_sum[h, 0:1] = mass
-            acc[h] = term
+                mass = mass + row_sum[h, 0:1, lanes] * fade
+                term = term + acc[h, :, lanes] * fade
+            row_max[h, 0:1, lanes] = top
+            row_sum[h, 0:1, lanes] = mass
+            acc[h, :, lanes] = term
+
+        tops = score(0)
+        for h in range(heads):
+            now = tops
+            if h + 1 < heads:
+                tops = score(h + 1)
+            mix(h, now)
+
+    def attend(e, diagonal):
+        prepare(e)
+        heads_over(diagonal)
 
     with scope("r_att0"):
         l_lgain.wait()
         l_up.wait()
         wait_crossed(0)
-        attend(0, True)
+        prepare(0)
+    with scope("p_relay1b"):
+        relay1(1)
+    with scope("r_att0_heads"):
+        heads_over(True)
+    with scope("t_relay3"):
+        if sp_count > 3:
+
+            @pl.when(sp >= 3)
+            def _():
+                arrived(3).wait_recv()
+                cross(3)
+
     with scope("s_att1"):
         if sp_count > 1:
 
@@ -426,40 +523,6 @@
                 wait_crossed(1)
                 attend(1, False)
 
-    with scope("t_relay3"):
-        if sp_count > 3:
-
-            @pl.when(sp >= 3)
-            def _():
-                arrived(3).wait_recv()
-                cross(3)
-
-    with scope("u_carrywait"):
-        for e in range(1, sp_count):
-
-            @pl.when(sp >= e)
-            def _(e=e):
-                carry_landed(e).wait_recv()
-
-            @pl.when(sp < e)
-            def _(e=e):
-                car_in[e - 1, 0:1] = jnp.ones((1, width), F32)
-                car_in[e - 1, 1:2] = jnp.zeros((1, width), F32)
-
-    with scope("v_rout"):
-        l_init.wait()
-        incoming = initial_state[...]
-        for e in range(sp_count - 1, 0, -1):
-            incoming = car_in[e - 1, 0:1] * incoming + car_in[e - 1, 1:2]
-        for c in range(width // LANES):
-            cols = slice(c * LANES, (c + 1) * LANES)
-            full = state[:, cols] + prod[:, cols] * incoming[:, cols]
-            rout[:, cols] = (full * jax.nn.silu(gate[:, cols].astype(F32))).astype(BF16)
-        l_rout.wait()
-        step = column_step(model)
-        for c in range(model // step):
-            cols = slice(c * step, (c + 1) * step)
-            racc[:, cols] = jnp.dot(rout[...], w_rout[:, cols], preferred_element_type=F32)
     with scope("w_att3"):
         if sp_count > 3:
 
@@ -484,20 +547,45 @@
 
             @pl.when(sp >= 2)
             def _():
-                arrived(2).wait_recv()
+                forwarded(0).wait_recv()
+                forwarded(1).wait_recv()
                 cross(2)
-                wait_crossed(2)
-
-    with scope("y_att2"):
-        if sp_count > 2:
-            pl.when(sp >= 2)(lambda: attend(2, False))
-    with scope("z_aout"):
-        for h in range(heads):
-            cols = slice(h * value, (h + 1) * value)
-            attended = (acc[h] * (1.0 / row_sum[h, 0:1])).T
-            aout[:, cols] = (attended * jax.nn.silu(attp[:, cols].astype(F32))).astype(BF16)
-
-    chunks, step = part.shape[1], part.shape[3]
+
+    with scope("u_carrywait"):
+        for e in range(1, sp_count):
+
+            @pl.when(sp >= e)
+            def _(e=e):
+                carry_landed(e).wait_recv()
+
+            @pl.when(sp < e)
+            def _(e=e):
+                row = lax.broadcasted_iota(jnp.int32, car_out.shape, 0)
+                car_in[e - 1] = jnp.where((row & 1) == 0, 1.0, 0.0)
+
+    with scope("v_rout"):
+        l_init.wait()
+        for c in range(width // LANES):
+            cols = slice(c * LANES, (c + 1) * LANES)
+            incoming = initial_state[:, cols]
+            for e in range(sp_count - 1, 0, -1):
+                incoming = (
+                    car_in[e - 1, 2 * c : 2 * c + 1] * incoming
+                    + car_in[e - 1, 2 * c + 1 : 2 * c + 2]
+                )
+            enter = segments[0:8, cols] * incoming + segments[8:16, cols]
+            full = state[c] + prod[c] * jnp.concatenate([enter] * long, axis=0)
+            mixed_rout[:, cols] = (full * silu_gate[:, cols]).astype(BF16)
+        rout[...] = jnp.dot(
+            unmixer[...], mixed_rout[...], preferred_element_type=F32
+        ).astype(BF16)
+        l_rout.wait()
+        step = column_step(model)
+        for c in range(model // step):
+            cols = slice(c * step, (c + 1) * step)
+            racc[:, cols] = jnp.dot(rout[...], w_rout[:, cols], preferred_element_type=F32)
+    chunks, step = part_in.shape[1], part_in.shape[3]
+    split = share % LANES == 0
 
     def part_copy(d, c):
         return remote(
@@ -510,12 +598,40 @@
         both = racc[here, cols] + jnp.dot(aout[here], w_aout[:, cols], preferred_element_type=F32)
         return both.astype(BF16)
 
-    with scope("z_outmm"):
+    def finish(here):
+        for h in range(heads):
+            cols = slice(h * value, (h + 1) * value)
+            attended = (acc[h, :, here] * (1.0 / row_sum[h, 0:1, here])).T
+            aout[here, cols] = (attended * jax.nn.silu(attp[here, cols].astype(F32))).astype(BF16)
+
+    def last(place):
+        if sp_count > 2:
+            pl.when(sp >= 2)(lambda: heads_over(False, share_rows(place), share))
+        finish(share_rows(place))
+
+    with scope("y_att2"):
+        if sp_count > 2:
+
+            @pl.when(sp >= 2)
+            def _():
+                wait_crossed(2)
+                prepare(2)
+                if not split:
+                    heads_over(False)
+
+        if not split:
+            finish(slice(None))
+    with scope("z_peer"):
         l_aout.wait()
-        for c in range(chunks):
-            for d in range(1, tp_count):
+        for d in range(1, tp_count):
+            if split:
+                last(peer(d))
+            for c in range(chunks):
                 part[d - 1, c] = partial(peer(d), c)
                 part_copy(d, c).start()
+    with scope("z_own"):
+        if split:
+            last(tp)
         for c in range(chunks):
             own_part[c] = partial(tp, c)
     with scope("z_sum"):
@@ -554,7 +670,11 @@
                     across(e, d).wait_send()
 
         if sp_count > 2:
-            pl.when((sp >= 1) & has_next)(lambda: forward().wait_send())
+
+            @pl.when((sp >= 1) & has_next)
+            def _():
+                forward(0).wait_send()
+                forward(1).wait_send()
 
 
 def body(
@@ -590,6 +710,8 @@
     dma = pltpu.SemaphoreType.DMA
     others = max(tp_count - 1, 1)
     hops = max(sp_count - 1, 1)
+    carries = -(-2 * width // LANES // 8) * 8
+    rims = -(-4 * width // LANES // 16) * 16
     pieces = 4 if share % 64 == 0 else 1
     chunks = 4 if model % (4 * LANES) == 0 else 1
     return pl.pallas_call(
@@ -607,17 +729,27 @@
             vmem((rows, taken), BF16),
             vmem((query_proj.shape[1], rows), BF16),
             vmem((heads, head_dim, rows), BF16),
-            vmem((16, width), BF16),
-            vmem((rows + 8, width), F32),
+            vmem((rims, LANES), BF16),
+            vmem((rims, LANES), BF16),
+            vmem((rows + 24, width), F32),
             vmem((LANES, LANES), BF16),
             vmem((LANES, LANES), BF16),
+            vmem((rows, rows), BF16),
+            vmem((rows, rows), BF16),
+            vmem((rows, LANES), F32),
             vmem((rows, width), F32),
-            vmem((rows, width), F32),
-            vmem((8, width), F32),
-            vmem((hops, 8, width), F32),
+            vmem((rows, width), BF16),
+            vmem((width // LANES, rows, LANES), F32),
+            vmem((width // LANES, rows, LANES), F32),
+            vmem((16, width), F32),
+            vmem((carries, LANES), F32),
+            vmem((hops, carries, LANES), F32),
             vmem((rows, width), BF16),
             vmem((rows, model), F32),
             vmem((rows, lat * tp_count), BF16),
+            vmem((rows, rope), BF16),
+            vmem((rows, latent_up.shape[1]), BF16),
+            vmem((heads, rows, rows), F32),
             vmem((heads, 8, rows), F32),
             vmem((heads, 8, rows), F32),
             vmem((heads, value, rows), F32),
@@ -626,7 +758,9 @@
             vmem((chunks, share, model // chunks), BF16),
             vmem((others, chunks, share, model // chunks), BF16),
             dma((len(hbm),)),
+            dma((pieces,)),
             dma((others, pieces)), dma((others, pieces)),
+            dma((2,)), dma((2,)),
             dma((2,)), dma((2,)),
             dma((hops,)), dma((hops,)),
             dma((sp_count, others)), dma((sp_count, others)),

time: 27.7 us -> 20.6 us (0.74)
  Pallas kernels: 26.8 us -> 19.6 us
    pallas_call x1, Pallas kernels: 26.8 us -> 19.6 us  [body(): pl.pallas_call(functools.partial(layer_kernel, sp_count, tp_count), out_s...]
where the time goes in v1:
time: 20.6 us; the launch traced here: 20.4 us
  Pallas kernels  19.6 us (95%)
  local copies, waits for them, and re-layouts  0.8 us (4%)
    pallas_call x1, Pallas kernels, body(): pl.pallas_call(functools.partial(layer_kernel, sp_count, tp_count), out_s...  19.6 us
    unnamed x1, local copies, waits for them, and re-layouts  0.8 us

profile of v1, /device:TPU:25, one launch (start us, length us, event | category | flops | bytes accessed | tf_op | source)
XLA Modules:
  0.0 20.4 jit_solution(7634318191847287073)
XLA Ops:
  0.0 19.6 %shard_map.199 = bf16[128,2048]{1,0:T(8,128)(2,1)S(1)} custom-call(bf16[128,2048]{1,0:T(8,128)(2,1)} %h_tokens.1, bf16[2048,256]{1,0:T(8,128)(2,1)} %h_lat.1, f32[1,2048]{1,0:T(1,128)} %bitcast.8, bf16[64,2048]{1,0:T(8,128)(2,1)} %bitcast.7, f32[8,128,128]{2,1,0:T(8,128)} %constant.4.clone.h_ktab, bf16[2048,512]{1,0:T(8,128)(2,1)} %h_in.1, ...), custom_call_target="tpu_custom_call" | custom-call | tf_op jit(solution)/shard_map/pallas_call | solution.py:717
  19.6 0.8 %copy.23 = bf16[128,2048]{1,0:T(8,128)(2,1)} copy(bf16[128,2048]{1,0:T(8,128)(2,1)S(1)} %shard_map.199) | data formatting | bytes 1048576

commit v2 on v1

--- a/solution.py
+++ b/solution.py
@@ -83,9 +83,9 @@
     w_up, initial_state, w_rout, w_aout,
     tok_all, normed, lat_all, sig, gate, attp, turned_q, queries, rim_out, rim_in, ext, diag_a, diag_b,
     mixer, unmixer, shift, silu_gate, mixed_rout,
-    prod, state, segments, car_out, car_in, rout, racc, xlat, rope_keys, kv, held, row_max, row_sum,
+    prod, state, segments, car_out, car_in, rout, racc, xlat, rope_keys, turned_v, kv, held, row_max, row_sum,
     acc, aout, part, own_part, part_in,
-    w_sem, tok_sem, tok_s, tok_r, z_s, z_r, y_s, y_r, fwd_s, fwd_r, l_s, l_r, rim_s, rim_r, c_s, c_r,
+    w_sem, tok_sem, tok_s, tok_r, z_s, z_r, y_s, y_r, fwd_s, fwd_r, l_s, l_r, x_s, x_r, rim_s, rim_r, c_s, c_r,
     p_s, p_r, ready,
 ):
     sp = lax.axis_index("sp")
@@ -226,6 +226,17 @@
         block = lat_all.at[sp - e, source(d)]
         return remote(block, block, l_s.at[e, d - 1], l_r.at[e, d - 1], tp=source(d))
 
+    def halves(k):
+        return (pl.ds(0, share), pl.ds(share, rows + tall - share))[k]
+
+    def across_piece(k, d):
+        block = lat_all.at[sp - 2, tp, halves(k)]
+        return remote(block, block, x_s.at[k, d - 1], x_r.at[k, d - 1], tp=peer(d))
+
+    def crossed_piece(k, d):
+        block = lat_all.at[sp - 2, source(d), halves(k)]
+        return remote(block, block, x_s.at[k, d - 1], x_r.at[k, d - 1], tp=source(d))
+
     def cross(e):
         for d in range(1, tp_count):
             across(e, d).start()
@@ -258,11 +269,6 @@
         keyed = (raw * key_table[:, :rope] + swapped * key_table[:, rope:]).astype(BF16)
         for k in range(packed):
             own[share : share + tall, k * rope : (k + 1) * rope] = keyed[k * tall : (k + 1) * tall]
-    with scope("e_in_own"):
-        for load in loads[6:8]:
-            load.start()
-        l_in.wait()
-        project(w_in, sig, share_rows(tp))
     with scope("g_norm_peer"):
         for k in range(pieces):
             for d in range(1, tp_count):
@@ -275,22 +281,22 @@
     def rim_landed():
         return remote(rim_out, rim_in, rim_s, rim_r, sp=sp - 1)
 
+    with scope("i_lat_b"):
+        for d in range(1, tp_count):
+            put_latent(d * share + tall, source(d))
+        pl.when(has_next)(lambda: along(1).start())
+        cross(0)
     with scope("h_in_peer"):
-        for load in loads[8:]:
+        for load in loads[6:]:
             load.start()
-        for d in range(1, tp_count):
-            project(w_in, sig, share_rows(source(d)))
+        l_in.wait()
+        project(w_in, sig)
         tail = sig[rows - 16 :].astype(F32)[12:]
         tail = [tail[:, c * LANES : (c + 1) * LANES] for c in range(width // LANES)]
         if len(tail) * 4 < rim_out.shape[0]:
             tail.append(jnp.zeros((rim_out.shape[0] - len(tail) * 4, LANES), F32))
         rim_out[...] = jnp.concatenate(tail, axis=0).astype(BF16)
         pl.when(has_next)(lambda: rim_copy().start())
-    with scope("i_lat_b"):
-        for d in range(1, tp_count):
-            put_latent(d * share + tall, source(d))
-        pl.when(has_next)(lambda: along(1).start())
-        cross(0)
     with scope("j_query"):
         l_query.wait()
         step = column_step(w_query.shape[1])
@@ -318,6 +324,27 @@
             queries[h, nope : nope + half] = (first * cosine - second * sine).astype(BF16)
             queries[h, nope + half :] = (first * sine + second * cosine).astype(BF16)
 
+    def relay1(k):
+        if sp_count > 1:
+
+            @pl.when(sp >= 1)
+            def _():
+                landed(k).wait_recv()
+                if sp_count > 2:
+                    pl.when(has_next)(lambda: forward(k).start())
+                if k:
+                    cross(1)
+
+    with scope("p_relay1a"):
+        relay1(0)
+
+    with scope("q_gates"):
+        l_gate.wait()
+        project(w_gate, gate)
+        silu_gate[...] = jax.nn.silu(
+            jnp.dot(mixer[...], gate[...], preferred_element_type=F32)
+        )
+
     with scope("l_direct"):
         for e in range(2, sp_count):
 
@@ -327,6 +354,12 @@
                 if e > 2:
                     direct(e).start()
 
+    with scope("q_gate_att"):
+        l_att.wait()
+        project(w_att, attp)
+
+    with scope("p_relay1b"):
+        relay1(1)
     with scope("m_rim"):
 
         @pl.when(sp == 0)
@@ -402,29 +435,6 @@
     with scope("o_carry"):
         for e in range(1, sp_count):
             pl.when(sp + e < sp_count)(lambda e=e: carry_copy(e).start())
-    def relay1(k):
-        if sp_count > 1:
-
-            @pl.when(sp >= 1)
-            def _():
-                landed(k).wait_recv()
-                if sp_count > 2:
-                    pl.when(has_next)(lambda: forward(k).start())
-                if k:
-                    cross(1)
-
-    with scope("p_relay1a"):
-        relay1(0)
-
-    with scope("q_gates"):
-        l_gate.wait()
-        project(w_gate, gate)
-        l_att.wait()
-        project(w_att, attp)
-        silu_gate[...] = jax.nn.silu(
-            jnp.dot(mixer[...], gate[...], preferred_element_type=F32)
-        )
-
     factor = head_dim ** (-0.5) * LOG2E
 
     def prepare(e):
@@ -453,46 +463,41 @@
         for c in range(w_up.shape[1] // step):
             cols = slice(c * step, (c + 1) * step)
             kv[:, cols] = jnp.dot(xlat[...], w_up[:, cols], preferred_element_type=F32).astype(BF16)
-
-    def heads_over(diagonal, lanes=slice(None), count=None):
-        count = rows if count is None else count
-
-        def score(h):
-            base = h * (nope + value)
-            keys = jnp.concatenate([kv[:, base : base + nope], rope_keys[...]], axis=1)
-            scores = jnp.dot(keys, queries[h, :, lanes], preferred_element_type=F32) * factor
-            if diagonal:
-                seen = lax.broadcasted_iota(jnp.int32, scores.shape, 0)
-                scores = jnp.where(
-                    seen <= lax.broadcasted_iota(jnp.int32, scores.shape, 1), scores, -jnp.inf
-                )
-            held[h, :, :count] = scores
-            return jnp.max(scores, axis=0, keepdims=True)
-
-        def mix(h, top):
+        for h in range(heads):
             base = h * (nope + value) + nope
-            if not diagonal:
-                before = row_max[h, 0:1, lanes]
-                top = jnp.maximum(top, before)
-                fade = jnp.exp2(before - top)
-            weights = jnp.exp2(held[h, :, :count] - top)
-            mass = jnp.sum(weights, axis=0, keepdims=True)
-            term = jnp.dot(
-                kv[:, base : base + value].T, weights.astype(BF16), preferred_element_type=F32
+            turned_v[h] = kv[:, base : base + value].T
+
+    def score(h, diagonal, lanes, count):
+        base = h * (nope + value)
+        keys = jnp.concatenate([kv[:, base : base + nope], rope_keys[...]], axis=1)
+        scores = jnp.dot(keys, queries[h, :, lanes], preferred_element_type=F32) * factor
+        if diagonal:
+            seen = lax.broadcasted_iota(jnp.int32, scores.shape, 0)
+            scores = jnp.where(
+                seen <= lax.broadcasted_iota(jnp.int32, scores.shape, 1), scores, -jnp.inf
             )
-            if not diagonal:
-                mass = mass + row_sum[h, 0:1, lanes] * fade
-                term = term + acc[h, :, lanes] * fade
-            row_max[h, 0:1, lanes] = top
-            row_sum[h, 0:1, lanes] = mass
-            acc[h, :, lanes] = term
-
-        tops = score(0)
+        held[h, :, :count] = scores
+        return jnp.max(scores, axis=0, keepdims=True)
+
+    def mix(h, top, diagonal, lanes, count):
+        if not diagonal:
+            before = row_max[h, 0:1, lanes]
+            top = jnp.maximum(top, before)
+            fade = jnp.exp2(before - top)
+        weights = jnp.exp2(held[h, :, :count] - top)
+        mass = jnp.sum(weights, axis=0, keepdims=True)
+        term = jnp.dot(turned_v[h], weights.astype(BF16), preferred_element_type=F32)
+        if not diagonal:
+            mass = mass + row_sum[h, 0:1, lanes] * fade
+            term = term + acc[h, :, lanes] * fade
+        row_max[h, 0:1, lanes] = top
+        row_sum[h, 0:1, lanes] = mass
+        acc[h, :, lanes] = term
+
+    def heads_over(diagonal, lanes=slice(None), count=rows):
+        tops = [score(h, diagonal, lanes, count) for h in range(heads)]
         for h in range(heads):
-            now = tops
-            if h + 1 < heads:
-                tops = score(h + 1)
-            mix(h, now)
+            mix(h, tops[h], diagonal, lanes, count)
 
     def attend(e, diagonal):
         prepare(e)
@@ -503,8 +508,6 @@
         l_up.wait()
         wait_crossed(0)
         prepare(0)
-    with scope("p_relay1b"):
-        relay1(1)
     with scope("r_att0_heads"):
         heads_over(True)
     with scope("t_relay3"):
@@ -547,9 +550,10 @@
 
             @pl.when(sp >= 2)
             def _():
-                forwarded(0).wait_recv()
-                forwarded(1).wait_recv()
-                cross(2)
+                for k in range(2):
+                    forwarded(k).wait_recv()
+                    for d in range(1, tp_count):
+                        across_piece(k, d).start()
 
     with scope("u_carrywait"):
         for e in range(1, sp_count):
@@ -604,36 +608,54 @@
             attended = (acc[h, :, here] * (1.0 / row_sum[h, 0:1, here])).T
             aout[here, cols] = (attended * jax.nn.silu(attp[here, cols].astype(F32))).astype(BF16)
 
-    def last(place):
-        if sp_count > 2:
-            pl.when(sp >= 2)(lambda: heads_over(False, share_rows(place), share))
-        finish(share_rows(place))
-
-    with scope("y_att2"):
-        if sp_count > 2:
-
-            @pl.when(sp >= 2)
-            def _():
-                wait_crossed(2)
-                prepare(2)
-                if not split:
-                    heads_over(False)
-
+    def send(d, c):
+        part[d - 1, c] = partial(peer(d), c)
+        part_copy(d, c).start()
+
+    def last_block():
+        for k in range(2):
+            for d in range(1, tp_count):
+                crossed_piece(k, d).wait_recv()
+        prepare(2)
         if not split:
+            heads_over(False)
             finish(slice(None))
-    with scope("z_peer"):
-        l_aout.wait()
+            for c in range(chunks):
+                for d in range(1, tp_count):
+                    send(d, c)
+            for c in range(chunks):
+                own_part[c] = partial(tp, c)
+            return
         for d in range(1, tp_count):
-            if split:
-                last(peer(d))
-            for c in range(chunks):
-                part[d - 1, c] = partial(peer(d), c)
-                part_copy(d, c).start()
-    with scope("z_own"):
-        if split:
-            last(tp)
+            heads_over(False, share_rows(peer(d)), share)
+            finish(share_rows(peer(d)))
+        mine = share_rows(tp)
+        sends = [(d, c) for d in range(1, tp_count) for c in range(chunks)]
+        each = -(-2 * len(sends) // heads)
+        tops = [score(h, False, mine, share) for h in range(heads)]
+        for h in range(heads):
+            for d, c in sends[h * each : (h + 1) * each]:
+                send(d, c)
+            mix(h, tops[h], False, mine, share)
+        finish(mine)
         for c in range(chunks):
             own_part[c] = partial(tp, c)
+
+    def no_block():
+        finish(slice(None))
+        for c in range(chunks):
+            for d in range(1, tp_count):
+                send(d, c)
+        for c in range(chunks):
+            own_part[c] = partial(tp, c)
+
+    with scope("y_last"):
+        l_aout.wait()
+        if sp_count > 2:
+            pl.when(sp >= 2)(last_block)
+            pl.when(sp < 2)(no_block)
+        else:
+            no_block()
     with scope("z_sum"):
         for c in range(chunks):
             summed = own_part[c].astype(F32)
@@ -667,7 +689,11 @@
             @pl.when(sp >= e)
             def _(e=e):
                 for d in range(1, tp_count):
-                    across(e, d).wait_send()
+                    if e == 2:
+                        across_piece(0, d).wait_send()
+                        across_piece(1, d).wait_send()
+                    else:
+                        across(e, d).wait_send()
 
         if sp_count > 2:
 
@@ -748,6 +774,7 @@
             vmem((rows, model), F32),
             vmem((rows, lat * tp_count), BF16),
             vmem((rows, rope), BF16),
+            vmem((heads, value, rows), BF16),
             vmem((rows, latent_up.shape[1]), BF16),
             vmem((heads, rows, rows), F32),
             vmem((heads, 8, rows), F32),
@@ -764,6 +791,7 @@
             dma((2,)), dma((2,)),
             dma((hops,)), dma((hops,)),
             dma((sp_count, others)), dma((sp_count, others)),
+            dma((2, others)), dma((2, others)),
             dma, dma,
             dma((hops,)), dma((hops,)),
             dma((others, chunks)), dma((others, chunks)),

time: 20.6 us -> 19.5 us (0.947)
  Pallas kernels: 19.6 us -> 18.5 us
    pallas_call x1, Pallas kernels: 19.6 us -> 18.5 us  [body(): pl.pallas_call(functools.partial(layer_kernel, sp_count, tp_count), out_s...]
where the time goes in v2:
time: 19.5 us; the launch traced here: 19.3 us
  Pallas kernels  18.5 us (95%)
  local copies, waits for them, and re-layouts  0.8 us (4%)
    pallas_call x1, Pallas kernels, body(): pl.pallas_call(functools.partial(layer_kernel, sp_count, tp_count), out_s...  18.5 us
    unnamed x1, local copies, waits for them, and re-layouts  0.8 us

profile of v2, /device:TPU:25, one launch (start us, length us, event | category | flops | bytes accessed | tf_op | source)
XLA Modules:
  0.0 19.3 jit_solution(703395161699162349)
XLA Ops:
  0.0 18.5 %shard_map.199 = bf16[128,2048]{1,0:T(8,128)(2,1)S(1)} custom-call(bf16[128,2048]{1,0:T(8,128)(2,1)} %h_tokens.1, bf16[2048,256]{1,0:T(8,128)(2,1)} %h_lat.1, f32[1,2048]{1,0:T(1,128)} %bitcast.8, bf16[64,2048]{1,0:T(8,128)(2,1)} %bitcast.7, f32[8,128,128]{2,1,0:T(8,128)} %constant.4.clone.h_ktab, bf16[2048,512]{1,0:T(8,128)(2,1)} %h_in.1, ...), custom_call_target="tpu_custom_call" | custom-call | tf_op jit(solution)/shard_map/pallas_call | solution.py:743
  18.5 0.8 %copy.23 = bf16[128,2048]{1,0:T(8,128)(2,1)} copy(bf16[128,2048]{1,0:T(8,128)(2,1)S(1)} %shard_map.199) | data formatting | bytes 1048576

commit v3 on v2

--- a/solution.py
+++ b/solution.py
@@ -85,7 +85,7 @@
     mixer, unmixer, shift, silu_gate, mixed_rout,
     prod, state, segments, car_out, car_in, rout, racc, xlat, rope_keys, turned_v, kv, held, row_max, row_sum,
     acc, aout, part, own_part, part_in,
-    w_sem, tok_sem, tok_s, tok_r, z_s, z_r, y_s, y_r, fwd_s, fwd_r, l_s, l_r, x_s, x_r, rim_s, rim_r, c_s, c_r,
+    w_sem, tok_s, tok_r, z_s, z_r, y_s, y_r, fwd_s, fwd_r, l_s, l_r, x_r, rim_s, rim_r, c_s, c_r,
     p_s, p_r, ready,
 ):
     sp = lax.axis_index("sp")
@@ -102,7 +102,7 @@
     value = w_att.shape[1] // heads
     packed = lat // rope
     tall = share // packed
-    pieces = tok_s.shape[1]
+    pieces = 4 if share % 64 == 0 else 1
     piece = share // pieces
     long = rows // 8
 
@@ -116,12 +116,13 @@
         conv_kernel, rec_blocks, inp_blocks, decay_rate, decay_shift, w_gate, w_att, latent_gain,
         w_up, initial_state, w_rout, w_aout,
     )
+    slots = (1, 2, 0, 3, 4, 5, 6, 0, 1, 4, 5, 0, 1, 6, 2, 3, 9, 7, 2, 3, 8)
     loads = [
-        pltpu.make_async_copy(a, b, w_sem.at[k]) for k, (a, b) in enumerate(zip(h_refs, w_refs)) if k
+        pltpu.make_async_copy(a, b, w_sem.at[k]) for a, b, k in zip(h_refs, w_refs, slots)
     ]
     token_loads = [
         pltpu.make_async_copy(
-            h_tokens.at[pl.ds(k * piece, piece)], tokens.at[pl.ds(k * piece, piece)], tok_sem.at[k]
+            h_tokens.at[pl.ds(k * piece, piece)], tokens.at[pl.ds(k * piece, piece)], w_sem.at[1]
         )
         for k in range(pieces)
     ]
@@ -135,25 +136,30 @@
     def greet(sem, **where):
         pl.semaphore_signal(sem, inc=1, device_id=where, device_id_type=pl.DeviceIdType.MESH)
 
+    (
+        l_tok, l_lat, l_norm, l_rope, l_ktab, l_in, l_query, l_qgain, l_qtab, l_conv, l_rec, l_inp,
+        l_rate, l_shift, l_gate, l_att, l_lgain, l_up, l_init, l_rout, l_aout,
+    ) = loads
     barrier = pltpu.get_barrier_semaphore()
     with scope("a_loads"):
         for d in range(1, tp_count):
             greet(barrier, tp=peer(d))
         for e in range(1, sp_count):
             pl.when(sp + e < sp_count)(lambda e=e: greet(barrier, sp=sp + e))
-        for load in [loads[1], *token_loads, loads[0]]:
+        l_norm.start()
+        for load in token_loads:
             load.start()
-    (
-        l_lat, l_norm, l_rope, l_ktab, l_in, l_query, l_qgain, l_qtab, l_conv, l_rec, l_inp,
-        l_rate, l_shift, l_gate, l_att, l_lgain, l_up, l_init, l_rout, l_aout,
-    ) = loads
+        l_lat.start()
 
     def token_copy(d, k):
         part_rows = pl.ds(k * piece, piece)
         return remote(
             h_tokens.at[part_rows], tok_all.at[d - 1, part_rows],
-            tok_s.at[d - 1, k], tok_r.at[d - 1, k], tp=peer(d),
+            tok_s.at[d - 1], tok_r.at[d - 1], tp=peer(d),
         )
+
+    def token_whole(d):
+        return remote(h_tokens, tok_all.at[d - 1], tok_s.at[d - 1], tok_r.at[d - 1], tp=peer(d))
 
     with scope("b_barrier"):
         pl.semaphore_wait(barrier, tp_count - 1 + sp)
@@ -162,7 +168,7 @@
                 token_copy(d, k).start()
         for e in range(1, sp_count):
             pl.when(sp >= e)(lambda e=e: greet(ready.at[e - 1], sp=sp - e))
-        for load in (loads[2], loads[3], loads[4], loads[5]):
+        for load in (l_rope, l_ktab, l_in, l_query):
             load.start()
 
     def share_rows(place):
@@ -187,8 +193,7 @@
     own = lat_all.at[sp, tp]
     with scope("c_norm_own"):
         l_norm.wait()
-        for k in range(pieces):
-            token_loads[k].wait()
+        l_tok.wait()
         put_normed(tokens[...], tp)
     with scope("d_lat_a"):
         l_lat.wait()
@@ -196,46 +201,45 @@
 
     def along(k):
         block = lat_all.at[sp, tp, (pl.ds(0, share), pl.ds(share, rows + tall - share))[k]]
-        return remote(block, block, z_s.at[k], z_r.at[k], sp=sp + 1)
+        return remote(block, block, z_s, z_r.at[k], sp=sp + 1)
 
     def landed(k):
         block = lat_all.at[sp - 1, tp, (pl.ds(0, share), pl.ds(share, rows + tall - share))[k]]
-        return remote(block, block, z_s.at[k], z_r.at[k], sp=sp - 1)
+        return remote(block, block, z_s, z_r.at[k], sp=sp - 1)
 
     def direct(e):
         block = lat_all.at[sp, tp]
-        return remote(block, block, fwd_s.at[e - 2], fwd_r.at[e - 2], sp=sp + e)
+        return remote(block, block, fwd_s.at[e - 3], fwd_r.at[e - 3], sp=sp + e)
 
     def forward(k):
         block = lat_all.at[sp - 1, tp, (pl.ds(0, share), pl.ds(share, rows + tall - share))[k]]
-        return remote(block, block, y_s.at[k], y_r.at[k], sp=sp + 1)
+        return remote(block, block, y_s, y_r.at[k], sp=sp + 1)
 
     def forwarded(k):
         block = lat_all.at[sp - 2, tp, (pl.ds(0, share), pl.ds(share, rows + tall - share))[k]]
-        return remote(block, block, y_s.at[k], y_r.at[k], sp=sp - 1)
+        return remote(block, block, y_s, y_r.at[k], sp=sp - 1)
 
     def arrived(e):
         block = lat_all.at[sp - e, tp]
-        return remote(block, block, fwd_s.at[e - 2], fwd_r.at[e - 2], sp=sp - 1)
+        return remote(block, block, fwd_s.at[e - 3], fwd_r.at[e - 3], sp=sp - 1)
+
+    def late(e):
+        return e if isinstance(e, int) and e < 2 else e - 1
 
     def across(e, d):
         block = lat_all.at[sp - e, tp]
-        return remote(block, block, l_s.at[e, d - 1], l_r.at[e, d - 1], tp=peer(d))
+        return remote(block, block, l_s.at[d - 1], l_r.at[late(e), d - 1], tp=peer(d))
 
     def crossed(e, d):
         block = lat_all.at[sp - e, source(d)]
-        return remote(block, block, l_s.at[e, d - 1], l_r.at[e, d - 1], tp=source(d))
+        return remote(block, block, l_s.at[d - 1], l_r.at[late(e), d - 1], tp=source(d))
 
     def halves(k):
         return (pl.ds(0, share), pl.ds(share, rows + tall - share))[k]
 
     def across_piece(k, d):
         block = lat_all.at[sp - 2, tp, halves(k)]
-        return remote(block, block, x_s.at[k, d - 1], x_r.at[k, d - 1], tp=peer(d))
-
-    def crossed_piece(k, d):
-        block = lat_all.at[sp - 2, source(d), halves(k)]
-        return remote(block, block, x_s.at[k, d - 1], x_r.at[k, d - 1], tp=source(d))
+        return remote(block, block, l_s.at[d - 1], x_r.at[d - 1], tp=peer(d))
 
     def cross(e):
         for d in range(1, tp_count):
@@ -270,10 +274,8 @@
         for k in range(packed):
             own[share : share + tall, k * rope : (k + 1) * rope] = keyed[k * tall : (k + 1) * tall]
     with scope("g_norm_peer"):
-        for k in range(pieces):
-            for d in range(1, tp_count):
-                token_copy(d, k).wait_recv()
         for d in range(1, tp_count):
+            token_whole(d).wait_recv()
             put_normed(tok_all[d - 1], source(d))
     def rim_copy():
         return remote(rim_out, rim_in, rim_s, rim_r, sp=sp + 1)
@@ -287,9 +289,9 @@
         pl.when(has_next)(lambda: along(1).start())
         cross(0)
     with scope("h_in_peer"):
-        for load in loads[6:]:
+        l_in.wait()
+        for load in (l_qgain, l_qtab, l_gate, l_att, l_conv, l_rec, l_up, l_lgain, l_aout):
             load.start()
-        l_in.wait()
         project(w_in, sig)
         tail = sig[rows - 16 :].astype(F32)[12:]
         tail = [tail[:, c * LANES : (c + 1) * LANES] for c in range(width // LANES)]
@@ -323,6 +325,8 @@
             queries[h, :nope] = head[:nope].astype(BF16)
             queries[h, nope : nope + half] = (first * cosine - second * sine).astype(BF16)
             queries[h, nope + half :] = (first * sine + second * cosine).astype(BF16)
+        for load in (l_inp, l_rate, l_shift):
+            load.start()
 
     def relay1(k):
         if sp_count > 1:
@@ -357,6 +361,8 @@
     with scope("q_gate_att"):
         l_att.wait()
         project(w_att, attp)
+        for load in (l_init, l_rout):
+            load.start()
 
     with scope("p_relay1b"):
         relay1(1)
@@ -427,10 +433,10 @@
             car_out[2 * c + 1 : 2 * c + 2] = two[7:8]
 
     def carry_copy(e):
-        return remote(car_out, car_in.at[e - 1], c_s.at[e - 1], c_r.at[e - 1], sp=sp + e)
+        return remote(car_out, car_in.at[e - 1], c_s, c_r, sp=sp + e)
 
     def carry_landed(e):
-        return remote(car_out, car_in.at[e - 1], c_s.at[e - 1], c_r.at[e - 1], sp=sp - e)
+        return remote(car_out, car_in.at[e - 1], c_s, c_r, sp=sp - e)
 
     with scope("o_carry"):
         for e in range(1, sp_count):
@@ -538,7 +544,7 @@
 
             def later(e, carry):
                 block = lat_all.at[sp - e, tp]
-                remote(block, block, fwd_s.at[e - 2], fwd_r.at[e - 2], sp=sp - 1).wait_recv()
+                remote(block, block, fwd_s.at[e - 3], fwd_r.at[e - 3], sp=sp - 1).wait_recv()
                 cross(e)
                 wait_crossed(e)
                 attend(e, False)
@@ -556,11 +562,13 @@
                         across_piece(k, d).start()
 
     with scope("u_carrywait"):
+        for v in range(1, sp_count):
+
+            @pl.when(sp == v)
+            def _(v=v):
+                remote(car_in.at[pl.ds(0, v)], car_in.at[pl.ds(0, v)], c_s, c_r, sp=sp - 1).wait_recv()
+
         for e in range(1, sp_count):
-
-            @pl.when(sp >= e)
-            def _(e=e):
-                carry_landed(e).wait_recv()
 
             @pl.when(sp < e)
             def _(e=e):
@@ -593,7 +601,7 @@
 
     def part_copy(d, c):
         return remote(
-            part.at[d - 1, c], part_in.at[d - 1, c], p_s.at[d - 1, c], p_r.at[d - 1, c], tp=peer(d)
+            part.at[d - 1, c], part_in.at[d - 1, c], p_s.at[d - 1], p_r.at[d - 1, c], tp=peer(d)
         )
 
     def partial(place, c):
@@ -613,9 +621,9 @@
         part_copy(d, c).start()
 
     def last_block():
-        for k in range(2):
-            for d in range(1, tp_count):
-                crossed_piece(k, d).wait_recv()
+        for d in range(1, tp_count):
+            block = lat_all.at[sp - 2, source(d)]
+            remote(block, block, l_s.at[d - 1], x_r.at[d - 1], tp=source(d)).wait_recv()
         prepare(2)
         if not split:
             heads_over(False)
@@ -666,41 +674,29 @@
 
     with scope("z_waits"):
         for d in range(1, tp_count):
-            for k in range(pieces):
-                token_copy(d, k).wait_send()
-            for c in range(chunks):
-                part_copy(d, c).wait_send()
-            across(0, d).wait_send()
-
-        @pl.when(has_next)
-        def _():
-            rim_copy().wait_send()
-            along(0).wait_send()
-            along(1).wait_send()
-
-        for e in range(1, sp_count):
-
-            @pl.when(sp + e < sp_count)
-            def _(e=e):
-                carry_copy(e).wait_send()
-                if e > 2:
+            token_whole(d).wait_send()
+            whole = part.at[d - 1]
+            remote(whole, whole, p_s.at[d - 1], p_r.at[d - 1, 0], tp=peer(d)).wait_send()
+
+        def all_sent(send, recv, count):
+            blocks = lat_all.at[pl.ds(0, count), 0]
+            remote(blocks, blocks, send, recv, tp=peer(1)).wait_send()
+
+        for v in range(sp_count):
+
+            @pl.when(sp == v)
+            def _(v=v):
+                for d in range(1, tp_count):
+                    all_sent(l_s.at[d - 1], l_r.at[0, d - 1], v + 1)
+                if v + 1 < sp_count:
+                    rim_copy().wait_send()
+                    all_sent(z_s, z_r.at[0], 1)
+                    if v and sp_count > 2:
+                        all_sent(y_s, y_r.at[0], 1)
+                    carries = car_in.at[pl.ds(0, sp_count - 1 - v)]
+                    remote(carries, carries, c_s, c_r, sp=sp + 1).wait_send()
+                for e in range(3, sp_count - v):
                     direct(e).wait_send()
-
-            @pl.when(sp >= e)
-            def _(e=e):
-                for d in range(1, tp_count):
-                    if e == 2:
-                        across_piece(0, d).wait_send()
-                        across_piece(1, d).wait_send()
-                    else:
-                        across(e, d).wait_send()
-
-        if sp_count > 2:
-
-            @pl.when((sp >= 1) & has_next)
-            def _():
-                forward(0).wait_send()
-                forward(1).wait_send()
 
 
 def body(
@@ -738,7 +734,6 @@
     hops = max(sp_count - 1, 1)
     carries = -(-2 * width // LANES // 8) * 8
     rims = -(-4 * width // LANES // 16) * 16
-    pieces = 4 if share % 64 == 0 else 1
     chunks = 4 if model % (4 * LANES) == 0 else 1
     return pl.pallas_call(
         functools.partial(layer_kernel, sp_count, tp_count),
@@ -784,17 +779,16 @@
             vmem((others, chunks, share, model // chunks), BF16),
             vmem((chunks, share, model // chunks), BF16),
             vmem((others, chunks, share, model // chunks), BF16),
-            dma((len(hbm),)),
-            dma((pieces,)),
-            dma((others, pieces)), dma((others, pieces)),
-            dma((2,)), dma((2,)),
-            dma((2,)), dma((2,)),
-            dma((hops,)), dma((hops,)),
-            dma((sp_count, others)), dma((sp_count, others)),
-            dma((2, others)), dma((2, others)),
+            dma((10,)),
+            dma((others,)), dma((others,)),
+            dma, dma((2,)),
+            dma, dma((2,)),
+            dma((max(sp_count - 3, 1),)), dma((max(sp_count - 3, 1),)),
+            dma((others,)), dma((max(sp_count - 1, 1), others)),
+            dma((others,)),
             dma, dma,
-            dma((hops,)), dma((hops,)),
-            dma((others, chunks)), dma((others, chunks)),
+            dma, dma,
+            dma((others,)), dma((others, chunks)),
             pltpu.SemaphoreType.REGULAR((hops,)),
         ],
         compiler_params=pltpu.CompilerParams(

time: 19.5 us -> 19.2 us (0.985)
  Pallas kernels: 18.5 us -> 18.1 us
    pallas_call x1, Pallas kernels: 18.5 us -> 18.1 us  [body(): pl.pallas_call(functools.partial(layer_kernel, sp_count, tp_count), out_s...]
where the time goes in v3:
time: 19.2 us; the launch traced here: 18.9 us
  Pallas kernels  18.1 us (94%)
  local copies, waits for them, and re-layouts  0.8 us (4%)
    pallas_call x1, Pallas kernels, body(): pl.pallas_call(functools.partial(layer_kernel, sp_count, tp_count), out_s...  18.1 us
    unnamed x1, local copies, waits for them, and re-layouts  0.8 us

profile of v3, /device:TPU:25, one launch (start us, length us, event | category | flops | bytes accessed | tf_op | source)
XLA Modules:
  0.0 18.9 jit_solution(6441348416345359797)
XLA Ops:
  0.0 18.1 %shard_map.199 = bf16[128,2048]{1,0:T(8,128)(2,1)S(1)} custom-call(bf16[128,2048]{1,0:T(8,128)(2,1)} %h_tokens.1, bf16[2048,256]{1,0:T(8,128)(2,1)} %h_lat.1, f32[1,2048]{1,0:T(1,128)} %bitcast.8, bf16[64,2048]{1,0:T(8,128)(2,1)} %bitcast.7, f32[8,128,128]{2,1,0:T(8,128)} %constant.4.clone.h_ktab, bf16[2048,512]{1,0:T(8,128)(2,1)} %h_in.1, ...), custom_call_target="tpu_custom_call" | custom-call | tf_op jit(solution)/shard_map/pallas_call | solution.py:738
  18.1 0.8 %copy.23 = bf16[128,2048]{1,0:T(8,128)(2,1)} copy(bf16[128,2048]{1,0:T(8,128)(2,1)S(1)} %shard_map.199) | data formatting | bytes 1048576

commit v4 on v3

--- a/solution.py
+++ b/solution.py
@@ -84,9 +84,9 @@
     tok_all, normed, lat_all, sig, gate, attp, turned_q, queries, rim_out, rim_in, ext, diag_a, diag_b,
     mixer, unmixer, shift, silu_gate, mixed_rout,
     prod, state, segments, car_out, car_in, rout, racc, xlat, rope_keys, turned_v, kv, held, row_max, row_sum,
-    acc, aout, part, own_part, part_in,
+    acc, aout, part, own_part, part_in, w_aout_in, w_rout_in, rout_in, aout_in, racc_in,
     w_sem, tok_s, tok_r, z_s, z_r, y_s, y_r, fwd_s, fwd_r, l_s, l_r, x_r, rim_s, rim_r, c_s, c_r,
-    p_s, p_r, ready,
+    p_s, p_r, wf_s, wf_r, ro_s, ro_r, ao_s, ao_r, ready,
 ):
     sp = lax.axis_index("sp")
     tp = lax.axis_index("tp")
@@ -158,6 +158,13 @@
             tok_s.at[d - 1], tok_r.at[d - 1], tp=peer(d),
         )
 
+    near = model // 2
+
+    def weight_copy(k, d):
+        source_ref = (h_aout, h_rout)[k].at[:, pl.ds(0, near)]
+        target_ref = (w_aout_in, w_rout_in)[k].at[d - 1]
+        return remote(source_ref, target_ref, wf_s.at[k, d - 1], wf_r.at[k, d - 1], tp=peer(d))
+
     def token_whole(d):
         return remote(h_tokens, tok_all.at[d - 1], tok_s.at[d - 1], tok_r.at[d - 1], tp=peer(d))
 
@@ -288,6 +295,8 @@
             put_latent(d * share + tall, source(d))
         pl.when(has_next)(lambda: along(1).start())
         cross(0)
+        for d in range(1, tp_count):
+            weight_copy(0, d).start()
     with scope("h_in_peer"):
         l_in.wait()
         for load in (l_qgain, l_qtab, l_gate, l_att, l_conv, l_rec, l_up, l_lgain, l_aout):
@@ -366,6 +375,8 @@
 
     with scope("p_relay1b"):
         relay1(1)
+        for d in range(1, tp_count):
+            weight_copy(1, d).start()
     with scope("m_rim"):
 
         @pl.when(sp == 0)
@@ -575,6 +586,16 @@
                 row = lax.broadcasted_iota(jnp.int32, car_out.shape, 0)
                 car_in[e - 1] = jnp.where((row & 1) == 0, 1.0, 0.0)
 
+    def rout_copy(d):
+        return remote(
+            rout.at[share_rows(peer(d))], rout_in.at[d - 1], ro_s.at[d - 1], ro_r.at[d - 1], tp=peer(d)
+        )
+
+    def aout_copy(d):
+        return remote(
+            aout.at[share_rows(peer(d))], aout_in.at[d - 1], ao_s.at[d - 1], ao_r.at[d - 1], tp=peer(d)
+        )
+
     with scope("v_rout"):
         l_init.wait()
         for c in range(width // LANES):
@@ -592,10 +613,16 @@
             unmixer[...], mixed_rout[...], preferred_element_type=F32
         ).astype(BF16)
         l_rout.wait()
-        step = column_step(model)
-        for c in range(model // step):
+        for d in range(1, tp_count):
+            rout_copy(d).start()
+        step = column_step(near)
+        for c in range(near // step):
+            cols = slice(near + c * step, near + (c + 1) * step)
+            racc[:, cols] = jnp.dot(rout[...], w_rout[:, cols], preferred_element_type=F32)
+        for c in range(near // step):
             cols = slice(c * step, (c + 1) * step)
-            racc[:, cols] = jnp.dot(rout[...], w_rout[:, cols], preferred_element_type=F32)
+            here = share_rows(tp)
+            racc[here, cols] = jnp.dot(rout[here], w_rout[:, cols], preferred_element_type=F32)
     chunks, step = part_in.shape[1], part_in.shape[3]
     split = share % LANES == 0
 
@@ -604,11 +631,28 @@
             part.at[d - 1, c], part_in.at[d - 1, c], p_s.at[d - 1], p_r.at[d - 1, c], tp=peer(d)
         )
 
-    def partial(place, c):
-        cols = slice(c * step, (c + 1) * step)
+    def partial(place, cols):
         here = share_rows(place)
         both = racc[here, cols] + jnp.dot(aout[here], w_aout[:, cols], preferred_element_type=F32)
         return both.astype(BF16)
+
+    def far(c):
+        return slice(near + c * step, near + (c + 1) * step)
+
+    def near_recurrent():
+        for d in range(1, tp_count):
+            rout_copy(d).wait_recv()
+            weight_copy(1, d).wait_recv()
+            for c in range(near // step):
+                cols = slice(c * step, (c + 1) * step)
+                racc_in[d - 1, :, cols] = jnp.dot(
+                    rout_in[d - 1], w_rout_in[d - 1, :, cols], preferred_element_type=F32
+                )
+
+    def own_rows():
+        for c in range(model // step):
+            cols = slice(c * step, (c + 1) * step)
+            own_part[:, cols] = partial(tp, cols)
 
     def finish(here):
         for h in range(heads):
@@ -617,8 +661,17 @@
             aout[here, cols] = (attended * jax.nn.silu(attp[here, cols].astype(F32))).astype(BF16)
 
     def send(d, c):
-        part[d - 1, c] = partial(peer(d), c)
+        part[d - 1, c] = partial(peer(d), far(c))
         part_copy(d, c).start()
+
+    def send_all():
+        for d in range(1, tp_count):
+            aout_copy(d).start()
+        for c in range(chunks):
+            for d in range(1, tp_count):
+                send(d, c)
+        near_recurrent()
+        own_rows()
 
     def last_block():
         for d in range(1, tp_count):
@@ -628,15 +681,12 @@
         if not split:
             heads_over(False)
             finish(slice(None))
-            for c in range(chunks):
-                for d in range(1, tp_count):
-                    send(d, c)
-            for c in range(chunks):
-                own_part[c] = partial(tp, c)
+            send_all()
             return
         for d in range(1, tp_count):
             heads_over(False, share_rows(peer(d)), share)
             finish(share_rows(peer(d)))
+            aout_copy(d).start()
         mine = share_rows(tp)
         sends = [(d, c) for d in range(1, tp_count) for c in range(chunks)]
         each = -(-2 * len(sends) // heads)
@@ -645,17 +695,13 @@
             for d, c in sends[h * each : (h + 1) * each]:
                 send(d, c)
             mix(h, tops[h], False, mine, share)
+        near_recurrent()
         finish(mine)
-        for c in range(chunks):
-            own_part[c] = partial(tp, c)
+        own_rows()
 
     def no_block():
         finish(slice(None))
-        for c in range(chunks):
-            for d in range(1, tp_count):
-                send(d, c)
-        for c in range(chunks):
-            own_part[c] = partial(tp, c)
+        send_all()
 
     with scope("y_last"):
         l_aout.wait()
@@ -665,16 +711,32 @@
         else:
             no_block()
     with scope("z_sum"):
+        for d in range(1, tp_count):
+            weight_copy(0, d).wait_recv()
+            aout_copy(d).wait_recv()
+        for c in range(near // step):
+            cols = slice(c * step, (c + 1) * step)
+            summed = own_part[:, cols].astype(F32)
+            for d in range(1, tp_count):
+                both = racc_in[d - 1, :, cols] + jnp.dot(
+                    aout_in[d - 1], w_aout_in[d - 1, :, cols], preferred_element_type=F32
+                )
+                summed = summed + both.astype(BF16).astype(F32)
+            out[:, cols] = summed.astype(BF16)
         for c in range(chunks):
-            summed = own_part[c].astype(F32)
+            summed = own_part[:, far(c)].astype(F32)
             for d in range(1, tp_count):
                 part_copy(d, c).wait_recv()
                 summed = summed + part_in[d - 1, c].astype(F32)
-            out[:, c * step : (c + 1) * step] = summed.astype(BF16)
+            out[:, far(c)] = summed.astype(BF16)
 
     with scope("z_waits"):
         for d in range(1, tp_count):
             token_whole(d).wait_send()
+            weight_copy(0, d).wait_send()
+            weight_copy(1, d).wait_send()
+            rout_copy(d).wait_send()
+            aout_copy(d).wait_send()
             whole = part.at[d - 1]
             remote(whole, whole, p_s.at[d - 1], p_r.at[d - 1, 0], tp=peer(d)).wait_send()
 
@@ -734,7 +796,7 @@
     hops = max(sp_count - 1, 1)
     carries = -(-2 * width // LANES // 8) * 8
     rims = -(-4 * width // LANES // 16) * 16
-    chunks = 4 if model % (4 * LANES) == 0 else 1
+    chunks = 2 if model % (4 * LANES) == 0 else 1
     return pl.pallas_call(
         functools.partial(layer_kernel, sp_count, tp_count),
         out_shape=pltpu.VMEM((share, model), BF16),
@@ -776,9 +838,14 @@
             vmem((heads, 8, rows), F32),
             vmem((heads, value, rows), F32),
             vmem((rows, taken), BF16),
-            vmem((others, chunks, share, model // chunks), BF16),
-            vmem((chunks, share, model // chunks), BF16),
-            vmem((others, chunks, share, model // chunks), BF16),
+            vmem((others, chunks, share, model // 2 // chunks), BF16),
+            vmem((share, model), BF16),
+            vmem((others, chunks, share, model // 2 // chunks), BF16),
+            vmem((others, taken, model // 2), BF16),
+            vmem((others, width, model // 2), BF16),
+            vmem((others, share, width), BF16),
+            vmem((others, share, taken), BF16),
+            vmem((others, share, model // 2), F32),
             dma((10,)),
             dma((others,)), dma((others,)),
             dma, dma((2,)),
@@ -789,6 +856,9 @@
             dma, dma,
             dma, dma,
             dma((others,)), dma((others, chunks)),
+            dma((2, others)), dma((2, others)),
+            dma((others,)), dma((others,)),
+            dma((others,)), dma((others,)),
             pltpu.SemaphoreType.REGULAR((hops,)),
         ],
         compiler_params=pltpu.CompilerParams(

time: 19.2 us -> 19 us (0.990)
  Pallas kernels: 18.1 us -> 17.9 us
    pallas_call x1, Pallas kernels: 18.1 us -> 17.9 us  [body(): pl.pallas_call(functools.partial(layer_kernel, sp_count, tp_count), out_s...]
where the time goes in v4:
time: 19 us; the launch traced here: 18.7 us
  Pallas kernels  17.9 us (94%)
  local copies, waits for them, and re-layouts  0.8 us (4%)
    pallas_call x1, Pallas kernels, body(): pl.pallas_call(functools.partial(layer_kernel, sp_count, tp_count), out_s...  17.9 us
    unnamed x1, local copies, waits for them, and re-layouts  0.8 us

profile of v4, /device:TPU:25, one launch (start us, length us, event | category | flops | bytes accessed | tf_op | source)
XLA Modules:
  0.0 18.7 jit_solution(14838134693418739139)
XLA Ops:
  0.0 17.9 %shard_map.199 = bf16[128,2048]{1,0:T(8,128)(2,1)S(1)} custom-call(bf16[128,2048]{1,0:T(8,128)(2,1)} %h_tokens.1, bf16[2048,256]{1,0:T(8,128)(2,1)} %h_lat.1, f32[1,2048]{1,0:T(1,128)} %bitcast.8, bf16[64,2048]{1,0:T(8,128)(2,1)} %bitcast.7, f32[8,128,128]{2,1,0:T(8,128)} %constant.4.clone.h_ktab, bf16[2048,512]{1,0:T(8,128)(2,1)} %h_in.1, ...), custom_call_target="tpu_custom_call" | custom-call | tf_op jit(solution)/shard_map/pallas_call | solution.py:800
  17.9 0.8 %copy.23 = bf16[128,2048]{1,0:T(8,128)(2,1)} copy(bf16[128,2048]{1,0:T(8,128)(2,1)S(1)} %shard_map.199) | data formatting | bytes 1048576

commit v5 on v4

--- a/solution.py
+++ b/solution.py
@@ -85,7 +85,7 @@
     mixer, unmixer, shift, silu_gate, mixed_rout,
     prod, state, segments, car_out, car_in, rout, racc, xlat, rope_keys, turned_v, kv, held, row_max, row_sum,
     acc, aout, part, own_part, part_in, w_aout_in, w_rout_in, rout_in, aout_in, racc_in,
-    w_sem, tok_s, tok_r, z_s, z_r, y_s, y_r, fwd_s, fwd_r, l_s, l_r, x_r, rim_s, rim_r, c_s, c_r,
+    w_sem, tok_s, tok_r, z_s, z_r, y_r, fwd_r, l_s, l_r, x_r, rim_s, rim_r, c_s, c_r,
     p_s, p_r, wf_s, wf_r, ro_s, ro_r, ao_s, ao_r, ready,
 ):
     sp = lax.axis_index("sp")
@@ -216,19 +216,19 @@
 
     def direct(e):
         block = lat_all.at[sp, tp]
-        return remote(block, block, fwd_s.at[e - 3], fwd_r.at[e - 3], sp=sp + e)
+        return remote(block, block, z_s, fwd_r.at[e - 3], sp=sp + e)
 
     def forward(k):
         block = lat_all.at[sp - 1, tp, (pl.ds(0, share), pl.ds(share, rows + tall - share))[k]]
-        return remote(block, block, y_s, y_r.at[k], sp=sp + 1)
+        return remote(block, block, z_s, y_r.at[k], sp=sp + 1)
 
     def forwarded(k):
         block = lat_all.at[sp - 2, tp, (pl.ds(0, share), pl.ds(share, rows + tall - share))[k]]
-        return remote(block, block, y_s, y_r.at[k], sp=sp - 1)
+        return remote(block, block, z_s, y_r.at[k], sp=sp - 1)
 
     def arrived(e):
         block = lat_all.at[sp - e, tp]
-        return remote(block, block, fwd_s.at[e - 3], fwd_r.at[e - 3], sp=sp - 1)
+        return remote(block, block, z_s, fwd_r.at[e - 3], sp=sp - 1)
 
     def late(e):
         return e if isinstance(e, int) and e < 2 else e - 1
@@ -354,11 +354,6 @@
     with scope("q_gates"):
         l_gate.wait()
         project(w_gate, gate)
-        silu_gate[...] = jax.nn.silu(
-            jnp.dot(mixer[...], gate[...], preferred_element_type=F32)
-        )
-
-    with scope("l_direct"):
         for e in range(2, sp_count):
 
             @pl.when(sp + e < sp_count)
@@ -366,6 +361,10 @@
                 pl.semaphore_wait(ready.at[e - 1], 1)
                 if e > 2:
                     direct(e).start()
+
+        silu_gate[...] = jax.nn.silu(
+            jnp.dot(mixer[...], gate[...], preferred_element_type=F32)
+        )
 
     with scope("q_gate_att"):
         l_att.wait()
@@ -555,7 +554,7 @@
 
             def later(e, carry):
                 block = lat_all.at[sp - e, tp]
-                remote(block, block, fwd_s.at[e - 3], fwd_r.at[e - 3], sp=sp - 1).wait_recv()
+                remote(block, block, z_s, fwd_r.at[e - 3], sp=sp - 1).wait_recv()
                 cross(e)
                 wait_crossed(e)
                 attend(e, False)
@@ -752,13 +751,10 @@
                     all_sent(l_s.at[d - 1], l_r.at[0, d - 1], v + 1)
                 if v + 1 < sp_count:
                     rim_copy().wait_send()
-                    all_sent(z_s, z_r.at[0], 1)
-                    if v and sp_count > 2:
-                        all_sent(y_s, y_r.at[0], 1)
+                    onward = int(v > 0 and sp_count > 2)
+                    all_sent(z_s, z_r.at[0], 1 + onward + max(sp_count - 3 - v, 0))
                     carries = car_in.at[pl.ds(0, sp_count - 1 - v)]
                     remote(carries, carries, c_s, c_r, sp=sp + 1).wait_send()
-                for e in range(3, sp_count - v):
-                    direct(e).wait_send()
 
 
 def body(
@@ -796,7 +792,7 @@
     hops = max(sp_count - 1, 1)
     carries = -(-2 * width // LANES // 8) * 8
     rims = -(-4 * width // LANES // 16) * 16
-    chunks = 2 if model % (4 * LANES) == 0 else 1
+    chunks = 1
     return pl.pallas_call(
         functools.partial(layer_kernel, sp_count, tp_count),
         out_shape=pltpu.VMEM((share, model), BF16),
@@ -849,8 +845,8 @@
             dma((10,)),
             dma((others,)), dma((others,)),
             dma, dma((2,)),
-            dma, dma((2,)),
-            dma((max(sp_count - 3, 1),)), dma((max(sp_count - 3, 1),)),
+            dma((2,)),
+            dma((max(sp_count - 3, 1),)),
             dma((others,)), dma((max(sp_count - 1, 1), others)),
             dma((others,)),
             dma, dma,

time: 19 us -> 18.8 us (0.989)
  Pallas kernels: 17.9 us -> 17.7 us
where the time goes in v5:
time: 18.8 us; the launch traced here: 18.5 us
  Pallas kernels  17.7 us (94%)
  local copies, waits for them, and re-layouts  0.8 us (4%)
    pallas_call x1, Pallas kernels, body(): pl.pallas_call(functools.partial(layer_kernel, sp_count, tp_count), out_s...  17.7 us
    unnamed x1, local copies, waits for them, and re-layouts  0.8 us

profile of v5, /device:TPU:25, one launch (start us, length us, event | category | flops | bytes accessed | tf_op | source)
XLA Modules:
  0.0 18.5 jit_solution(6955405181166723668)
XLA Ops:
  0.0 17.7 %shard_map.199 = bf16[128,2048]{1,0:T(8,128)(2,1)S(1)} custom-call(bf16[128,2048]{1,0:T(8,128)(2,1)} %h_tokens.1, bf16[2048,256]{1,0:T(8,128)(2,1)} %h_lat.1, f32[1,2048]{1,0:T(1,128)} %bitcast.8, bf16[64,2048]{1,0:T(8,128)(2,1)} %bitcast.7, f32[8,128,128]{2,1,0:T(8,128)} %constant.4.clone.h_ktab, bf16[2048,512]{1,0:T(8,128)(2,1)} %h_in.1, ...), custom_call_target="tpu_custom_call" | custom-call | tf_op jit(solution)/shard_map/pallas_call | solution.py:796
  17.7 0.8 %copy.23 = bf16[128,2048]{1,0:T(8,128)(2,1)} copy(bf16[128,2048]{1,0:T(8,128)(2,1)S(1)} %shard_map.199) | data formatting | bytes 1048576

commit v6 on v5

--- a/solution.py
+++ b/solution.py
@@ -82,7 +82,7 @@
     conv_kernel, rec_blocks, inp_blocks, decay_rate, decay_shift, w_gate, w_att, latent_gain,
     w_up, initial_state, w_rout, w_aout,
     tok_all, normed, lat_all, sig, gate, attp, turned_q, queries, rim_out, rim_in, ext, diag_a, diag_b,
-    mixer, unmixer, shift, silu_gate, mixed_rout,
+    mixer, unmixer, shift, silu_gate, silu_att, mixed_rout,
     prod, state, segments, car_out, car_in, rout, racc, xlat, rope_keys, turned_v, kv, held, row_max, row_sum,
     acc, aout, part, own_part, part_in, w_aout_in, w_rout_in, rout_in, aout_in, racc_in,
     w_sem, tok_s, tok_r, z_s, z_r, y_r, fwd_r, l_s, l_r, x_r, rim_s, rim_r, c_s, c_r,
@@ -376,6 +376,7 @@
         relay1(1)
         for d in range(1, tp_count):
             weight_copy(1, d).start()
+    silu_att[...] = jax.nn.silu(attp[...].astype(F32)).T
     with scope("m_rim"):
 
         @pl.when(sp == 0)
@@ -656,8 +657,8 @@
     def finish(here):
         for h in range(heads):
             cols = slice(h * value, (h + 1) * value)
-            attended = (acc[h, :, here] * (1.0 / row_sum[h, 0:1, here])).T
-            aout[here, cols] = (attended * jax.nn.silu(attp[here, cols].astype(F32))).astype(BF16)
+            attended = acc[h, :, here] * (1.0 / row_sum[h, 0:1, here])
+            aout[here, cols] = (attended * silu_att[cols, here]).astype(BF16).T
 
     def send(d, c):
         part[d - 1, c] = partial(peer(d), far(c))
@@ -817,6 +818,7 @@
             vmem((rows, rows), BF16),
             vmem((rows, LANES), F32),
             vmem((rows, width), F32),
+            vmem((taken, rows), F32),
             vmem((rows, width), BF16),
             vmem((width // LANES, rows, LANES), F32),
             vmem((width // LANES, rows, LANES), F32),

time: 18.8 us -> 18.7 us (level)
  no operation moved by 1% of the time
where the time goes in v6:
time: 18.7 us; the launch traced here: 18.5 us
  Pallas kernels  17.7 us (95%)
  local copies, waits for them, and re-layouts  0.8 us (4%)
    pallas_call x1, Pallas kernels, body(): pl.pallas_call(functools.partial(layer_kernel, sp_count, tp_count), out_s...  17.7 us
    unnamed x1, local copies, waits for them, and re-layouts  0.8 us

profile of v6, /device:TPU:25, one launch (start us, length us, event | category | flops | bytes accessed | tf_op | source)
XLA Modules:
  0.0 18.5 jit_solution(11350523490897876109)
XLA Ops:
  0.0 17.7 %shard_map.199 = bf16[128,2048]{1,0:T(8,128)(2,1)S(1)} custom-call(bf16[128,2048]{1,0:T(8,128)(2,1)} %h_tokens.1, bf16[2048,256]{1,0:T(8,128)(2,1)} %h_lat.1, f32[1,2048]{1,0:T(1,128)} %bitcast.8, bf16[64,2048]{1,0:T(8,128)(2,1)} %bitcast.7, f32[8,128,128]{2,1,0:T(8,128)} %constant.4.clone.h_ktab, bf16[2048,512]{1,0:T(8,128)(2,1)} %h_in.1, ...), custom_call_target="tpu_custom_call" | custom-call | tf_op jit(solution)/shard_map/pallas_call | solution.py:797
  17.7 0.8 %copy.23 = bf16[128,2048]{1,0:T(8,128)(2,1)} copy(bf16[128,2048]{1,0:T(8,128)(2,1)S(1)} %shard_map.199) | data formatting | bytes 1048576
